TPU v7x, 256 devices: a whole 4x4x8 slice. The times are simulated.
256 devices in a mesh: kv: 32 (over z, y), tp: 8 (over x, core).
Axes of the slice: x: 4, y: 4, z: 8, core: 2. Of those that a mesh axis runs over, the one named last changes fastest.
Arguments:
- piece_tokens: bfloat16 [3072, 4096], P('kv'), may hold values from -6 to 6
- step_tokens: bfloat16 [32, 4096], P('kv'), may hold values from -6 to 6
- in_gain: float32 [4096], replicated, may hold values from 0.1 to 1.9
- w_query: bfloat16 [4096, 8, 2, 128], P(None, 'tp'), may hold values from -0.09375 to 0.09375
- w_key: bfloat16 [4096, 8, 2, 128], P(None, 'tp'), may hold values from -0.15625 to 0.15625
- w_value: bfloat16 [4096, 8, 256], P(None, 'tp'), may hold values from -0.09375 to 0.09375
- w_out: bfloat16 [8, 256, 4096], P('tp'), may hold values from -0.125 to 0.125
- mix_ratio: float32 [8], P('tp'), may hold values from 0.3 to 0.8
- out_gain: float32 [256], replicated, may hold values from 0.1 to 1.9
- prompt_keys: bfloat16 [65536, 8, 2, 128], P('kv', 'tp'), may hold values from -630 to 630
- prompt_values: bfloat16 [65536, 8, 256], P('kv', 'tp'), may hold values from -6 to 6
- step_cache_keys: bfloat16 [32, 4096, 8, 2, 128], P(None, 'kv', 'tp'), may hold values from -630 to 630
- step_cache_values: bfloat16 [32, 4096, 8, 256], P(None, 'kv', 'tp'), may hold values from -6 to 6
- prompt_len: int32 [1], replicated, may hold values from 64512 to 65536
- step_lens: int32 [32], replicated, may hold values from 4032 to 4096
Outputs:
- piece_out: bfloat16 [3072, 4096], P('kv', 'tp')
- step_out: bfloat16 [32, 4096], P('kv', 'tp')
- piece_keys: bfloat16 [3072, 8, 2, 128], P('kv', 'tp')
- piece_values: bfloat16 [3072, 8, 256], P('kv', 'tp')
- step_keys: bfloat16 [32, 8, 2, 128], P('kv', 'tp')
- step_values: bfloat16 [32, 8, 256], P('kv', 'tp')
Inputs may be any that keep to these rules, and one draw needn't show every extreme that they name: `prompt_len`: the piece's tokens follow these cached positions. `step_lens`: each decoding token follows its sequence's cached positions.
All inputs are finite; a program needn't handle non-finite values.
Results may differ from a plain program's by a relative error of at most 0.015.
Values may be sent and summed in bfloat16 or wider, within the bound.
A program may use at most 128 MiB of HBM per device.

v0:
```python
import functools
import math

import jax
import jax.numpy as jnp
from jax import lax
from jax.experimental import pallas as pl
from jax.experimental.pallas import tpu as pltpu
from jax.sharding import PartitionSpec as P

EPS = 1e-06
OUT_SCALE = 0.8
MESH = pl.DeviceIdType.MESH
HIDDEN = -1e30


def norm_rows(tokens, in_gain):
    floats = tokens.astype(jnp.float32)
    inv_rms = lax.rsqrt(jnp.mean(floats * floats, axis=-1, keepdims=True) + EPS)
    return (floats * inv_rms * in_gain).astype(jnp.bfloat16)


def project(normed, weight):
    order = tuple(range(1, weight.ndim - 1)) + (0, weight.ndim - 1)
    parts = jnp.transpose(weight, order)
    parts = parts.reshape((-1,) + parts.shape[-2:])
    product = jnp.einsum("nd,gdk->gnk", normed, parts, preferred_element_type=jnp.float32)
    return product.astype(jnp.bfloat16)


def meet(axis, count):
    me = lax.axis_index(axis)
    barrier = pltpu.get_barrier_semaphore()
    for step in range(1, count):
        pl.semaphore_signal(
            barrier, inc=1, device_id={axis: lax.rem(me + step, count)}, device_id_type=MESH
        )
    pl.semaphore_wait(barrier, count - 1)
    return me


def gather_kernel(axis, count, own, everyone, send_sem, recv_sem):
    me = meet(axis, count)
    copies = []
    for step in range(1, count):
        copy = pltpu.make_async_remote_copy(
            src_ref=own,
            dst_ref=everyone.at[me],
            send_sem=send_sem.at[step],
            recv_sem=recv_sem.at[step],
            device_id={axis: lax.rem(me + step, count)},
            device_id_type=MESH,
        )
        copy.start()
        copies.append(copy)
    everyone[me] = own[...]
    for copy in copies:
        copy.wait()


def gather_rows(own, axis, count, collective):
    return pl.pallas_call(
        functools.partial(gather_kernel, axis, count),
        out_shape=jax.ShapeDtypeStruct((count,) + own.shape, own.dtype),
        in_specs=[pl.BlockSpec(memory_space=pltpu.VMEM)],
        out_specs=pl.BlockSpec(memory_space=pltpu.VMEM),
        scratch_shapes=[
            pltpu.SemaphoreType.DMA((count,)),
            pltpu.SemaphoreType.DMA((count,)),
        ],
        compiler_params=pltpu.CompilerParams(collective_id=collective, has_side_effects=True),
        name="gather_rows",
    )(own)


def attend_kernel(rows, dims, q_ref, k_ref, v_ref, fk_ref, fv_ref, bias_ref, own_ref, o_ref, s_ref):
    part = pl.program_id(1)
    owners = q_ref.shape[0]
    scale = dims ** (-0.5)
    fold = scale * math.log2(math.e)
    q = q_ref[:, :rows, :].reshape(owners * rows, dims)
    contract = (((1,), (1,)), ((), ()))
    old = lax.dot_general(q, k_ref[0], contract, preferred_element_type=jnp.float32)
    old = old + bias_ref[...]
    new = lax.dot_general(q, fk_ref[0], contract, preferred_element_type=jnp.float32)
    place = pl.program_id(0) * owners * rows + lax.broadcasted_iota(jnp.int32, new.shape, 0)
    new = jnp.where(own_ref[...] <= place, new, HIDDEN)
    top = jnp.maximum(
        jnp.max(old, axis=1, keepdims=True), jnp.max(new, axis=1, keepdims=True)
    )
    old_w = jnp.exp2((old - top) * fold)
    new_w = jnp.exp2((new - top) * fold)
    total = jnp.sum(old_w, axis=1, keepdims=True) + jnp.sum(new_w, axis=1, keepdims=True)
    summed = jnp.dot(old_w.astype(jnp.bfloat16), v_ref[0], preferred_element_type=jnp.float32)
    summed += jnp.dot(new_w.astype(jnp.bfloat16), fv_ref[0], preferred_element_type=jnp.float32)
    o_ref[...] = summed.astype(jnp.bfloat16).reshape(o_ref.shape)
    parts = pl.num_programs(1)
    lane = lax.broadcasted_iota(jnp.int32, (owners * rows, s_ref.shape[-1]), 1)
    put = jnp.where(lane == part, top * scale, jnp.where(lane == parts + part, total, 0.0))
    put = put.reshape(s_ref.shape)

    @pl.when(part == 0)
    def _():
        s_ref[...] = put

    @pl.when(part != 0)
    def _():
        s_ref[...] += put


def attend(q_all, keys, values, fresh_k, fresh_v, bias, fresh_place, rows):
    count, padded, _ = q_all.shape
    parts, cached, dims = keys.shape
    maps = parts // values.shape[0]
    wide = values.shape[-1]
    owners = math.gcd(count, 2)
    return pl.pallas_call(
        functools.partial(attend_kernel, rows, dims),
        grid=(count // owners, parts),
        in_specs=[
            pl.BlockSpec((owners, padded, dims), lambda i, p: (i, 0, p)),
            pl.BlockSpec((1, cached, dims), lambda i, p: (p, 0, 0)),
            pl.BlockSpec((1, cached, wide), lambda i, p: (p // maps, 0, 0)),
            pl.BlockSpec((1, rows, dims), lambda i, p: (p, 0, 0)),
            pl.BlockSpec((1, rows, wide), lambda i, p: (p // maps, 0, 0)),
            pl.BlockSpec((1, cached), lambda i, p: (0, 0)),
            pl.BlockSpec((1, rows), lambda i, p: (0, 0)),
        ],
        out_specs=[
            pl.BlockSpec((owners, rows, wide), lambda i, p: (i, 0, p)),
            pl.BlockSpec((owners, rows, 128), lambda i, p: (i, 0, 0)),
        ],
        out_shape=[
            jax.ShapeDtypeStruct((count, rows, parts * wide), jnp.bfloat16),
            jax.ShapeDtypeStruct((count, rows, 128), jnp.float32),
        ],
        compiler_params=pltpu.CompilerParams(
            dimension_semantics=("arbitrary", "arbitrary"), vmem_limit_bytes=56 * 1024 * 1024
        ),
        name="attend",
    )(q_all, keys, values, fresh_k, fresh_v, bias, fresh_place)


def mix_maps(first, second, ratio, gain):
    mixed = first - ratio * second
    inv_rms = lax.rsqrt(jnp.mean(mixed * mixed, axis=-1, keepdims=True) + EPS)
    return (mixed * inv_rms * gain * OUT_SCALE).astype(jnp.bfloat16)


def blend(values, tops, totals):
    count = len(values)
    best = functools.reduce(jnp.maximum, tops)
    scales = [jnp.exp(top - best) for top in tops]
    norm = functools.reduce(jnp.add, [scales[g] * totals[g] for g in range(count)])
    total = functools.reduce(jnp.add, [values[g] * scales[g] for g in range(count)])
    return total / norm


def exchange_kernel(
    axis, count, parts, maps, wide, ratio, gain, vals, stats, step, out, all_v, all_s, all_t, send_sem, recv_sem
):
    me = meet(axis, count)
    copies = []
    for turn in range(1, count):
        other = lax.rem(me + turn, count)
        for slot, (mine, theirs) in enumerate(((stats, all_s), (step, all_t), (vals, all_v))):
            copy = pltpu.make_async_remote_copy(
                src_ref=mine.at[other],
                dst_ref=theirs.at[me],
                send_sem=send_sem.at[turn, slot],
                recv_sem=recv_sem.at[turn, slot],
                device_id={axis: other},
                device_id_type=MESH,
            )
            copy.start()
            copies.append(copy)
    all_v[me] = vals[me]
    all_s[me] = stats[me]
    all_t[me] = step[me]
    for copy in copies:
        copy.wait()
    rows = vals.shape[1]
    steps = step.shape[1] // parts
    out[...] = jnp.zeros_like(out)
    tall = math.gcd(rows, 32)

    def chunk(index, carry):
        at = pl.ds(pl.multiple_of(index * tall, tall), tall)
        for head in range(parts // maps):
            maps_out = []
            for part in range(head * maps, head * maps + maps):
                cut = slice(part * wide, part * wide + wide)
                maps_out.append(
                    blend(
                        [all_v[g, at, cut].astype(jnp.float32) for g in range(count)],
                        [all_s[g, at, part : part + 1] for g in range(count)],
                        [all_s[g, at, parts + part : parts + part + 1] for g in range(count)],
                    )
                )
            out[at, head * wide : head * wide + wide] = mix_maps(
                maps_out[0], maps_out[1], ratio[0, head], gain[...]
            )
        return carry

    lax.fori_loop(0, rows // tall, chunk, 0)
    low = out.shape[0] - rows
    for head in range(parts // maps):
        lines = []
        for seq in range(steps):
            maps_out = []
            for part in range(seq * parts + head * maps, seq * parts + head * maps + maps):
                line = [all_t[g, part : part + 1, :] for g in range(count)]
                maps_out.append(
                    blend(
                        [v[:, :wide] for v in line],
                        [v[:, wide : wide + 1] for v in line],
                        [v[:, wide + 1 : wide + 2] for v in line],
                    )
                )
            lines.append(mix_maps(maps_out[0], maps_out[1], ratio[0, head], gain[...]).astype(jnp.float32))
        place = lax.broadcasted_iota(jnp.int32, (low, wide), 0)
        block = jnp.zeros((low, wide), jnp.float32)
        for seq in range(steps):
            block = jnp.where(place == seq, lines[seq], block)
        out[rows:, head * wide : head * wide + wide] = block.astype(jnp.bfloat16)


def exchange(values, stats, step, ratio, gain, axis, count, maps, padded, collective):
    parts = values.shape[-1] // gain.shape[-1]
    wide = gain.shape[-1]
    vmem = pl.BlockSpec(memory_space=pltpu.VMEM)
    return pl.pallas_call(
        functools.partial(exchange_kernel, axis, count, parts, maps, wide),
        out_shape=jax.ShapeDtypeStruct((padded, parts // maps * wide), jnp.bfloat16),
        in_specs=[pl.BlockSpec(memory_space=pltpu.SMEM), vmem, vmem, vmem, vmem],
        out_specs=vmem,
        scratch_shapes=[
            pltpu.VMEM(values.shape, values.dtype),
            pltpu.VMEM(stats.shape, stats.dtype),
            pltpu.VMEM(step.shape, step.dtype),
            pltpu.SemaphoreType.DMA((count, 3)),
            pltpu.SemaphoreType.DMA((count, 3)),
        ],
        compiler_params=pltpu.CompilerParams(
            collective_id=collective, has_side_effects=True, vmem_limit_bytes=56 * 1024 * 1024
        ),
        name="exchange",
    )(ratio, gain, values, stats, step)


def project_out_kernel(axis, count, heads, weight, out, terms, pair, half, far, d_send, d_recv, x_send, x_recv):
    me = lax.axis_index(axis)
    chips = count // 2
    chip, core = me // 2, lax.rem(me, 2)
    meet(axis, count)
    wide = out.shape[1]
    for target in range(count):
        terms[target] = jnp.dot(
            heads[...], weight[:, target * wide : target * wide + wide], preferred_element_type=jnp.float32
        ).astype(jnp.bfloat16)
    near = []
    for turn in range(1, chips + 1):
        there = lax.rem(chip + turn, chips)
        copy = pltpu.make_async_remote_copy(
            src_ref=terms.at[there * 2 + 1 - core],
            dst_ref=pair.at[there],
            send_sem=d_send.at[turn],
            recv_sem=d_recv.at[turn],
            device_id={axis: chip * 2 + 1 - core},
            device_id_type=MESH,
        )
        copy.start()
        near.append(copy)
    away = []
    for turn in range(1, chips + 1):
        near[turn - 1].wait()
        there = lax.rem(chip + turn, chips)
        both = terms[there * 2 + core].astype(jnp.float32) + pair[there].astype(jnp.float32)
        if turn == chips:
            total = both
            for copy in away:
                copy.wait()
            for slot in range(1, chips):
                total = total + far[slot].astype(jnp.float32)
            out[...] = total.astype(jnp.bfloat16)
        else:
            half[turn] = both.astype(jnp.bfloat16)
            copy = pltpu.make_async_remote_copy(
                src_ref=half.at[turn],
                dst_ref=far.at[turn],
                send_sem=x_send.at[turn],
                recv_sem=x_recv.at[turn],
                device_id={axis: there * 2 + core},
                device_id_type=MESH,
            )
            copy.start()
            away.append(copy)


def project_out(heads, weight, axis, count, collective):
    wide = weight.shape[1] // count
    rows = heads.shape[0]
    chips = count // 2
    vmem = pl.BlockSpec(memory_space=pltpu.VMEM)
    return pl.pallas_call(
        functools.partial(project_out_kernel, axis, count),
        out_shape=jax.ShapeDtypeStruct((rows, wide), jnp.bfloat16),
        in_specs=[vmem, vmem],
        out_specs=vmem,
        scratch_shapes=[
            pltpu.VMEM((count, rows, wide), jnp.bfloat16),
            pltpu.VMEM((chips, rows, wide), jnp.bfloat16),
            pltpu.VMEM((chips, rows, wide), jnp.bfloat16),
            pltpu.VMEM((chips, rows, wide), jnp.bfloat16),
            pltpu.SemaphoreType.DMA((chips + 1,)),
            pltpu.SemaphoreType.DMA((chips + 1,)),
            pltpu.SemaphoreType.DMA((chips + 1,)),
            pltpu.SemaphoreType.DMA((chips + 1,)),
        ],
        compiler_params=pltpu.CompilerParams(
            collective_id=collective, has_side_effects=True, vmem_limit_bytes=56 * 1024 * 1024
        ),
        name="project_out",
    )(heads, weight)


def on_device(
    kv_count,
    tp_count,
    piece_tokens,
    step_tokens,
    in_gain,
    w_query,
    w_key,
    w_value,
    w_out,
    mix_ratio,
    out_gain,
    prompt_keys,
    prompt_values,
    step_cache_keys,
    step_cache_values,
    prompt_len,
    step_lens,
):
    kv_place = lax.axis_index("kv")
    piece_dev = piece_tokens.shape[0]
    step_dev = step_tokens.shape[0]
    cache_dev = prompt_keys.shape[0]
    seq_count = step_cache_keys.shape[0]
    seq_cache = step_cache_keys.shape[1]
    heads, maps, dims = w_query.shape[1:]
    wide = w_value.shape[-1]
    parts = heads * maps
    padded = -(-(piece_dev + step_dev) // 16) * 16
    spare = jnp.zeros((padded - piece_dev - step_dev, piece_tokens.shape[1]), jnp.bfloat16)
    all_rows = jnp.concatenate([piece_tokens, step_tokens, spare], axis=0)
    normed = norm_rows(all_rows, in_gain)
    queries = project(normed, w_query)
    key_rows = project(normed, w_key)
    value_rows = project(normed, w_value)
    q_flat = jnp.transpose(queries, (1, 0, 2)).reshape(padded, parts * dims)
    q_all = gather_rows(q_flat, "kv", kv_count, 0)
    end = piece_dev + step_dev

    def rows_of(flat, start, stop, extra):
        return jnp.transpose(flat[:, start:stop], (1, 0, 2)).reshape((stop - start,) + extra)

    piece_k = rows_of(key_rows, 0, piece_dev, (heads, maps, dims))
    step_k = rows_of(key_rows, piece_dev, end, (heads, maps, dims))
    piece_v = rows_of(value_rows, 0, piece_dev, (heads, wide))
    step_v = rows_of(value_rows, piece_dev, end, (heads, wide))
    keys = jnp.transpose(prompt_keys, (1, 2, 0, 3)).reshape(parts, cache_dev, dims)
    values = jnp.transpose(prompt_values, (1, 0, 2))
    cache_ok = kv_place * cache_dev + jnp.arange(cache_dev, dtype=jnp.int32) < prompt_len[0]
    bias = jnp.where(cache_ok, 0.0, HIDDEN)[None, :]
    fresh_place = (kv_place * piece_dev + jnp.arange(piece_dev, dtype=jnp.int32))[None, :]
    piece_sum, piece_stats = attend(
        q_all,
        keys,
        values,
        key_rows[:, :piece_dev],
        value_rows[:, :piece_dev],
        bias,
        fresh_place,
        piece_dev,
    )
    step_q = q_all[:, piece_dev:end].reshape(seq_count, heads, maps, dims)
    own_seq = jnp.arange(seq_count, dtype=jnp.int32) // step_dev == kv_place
    own_k = lax.dynamic_update_slice_in_dim(
        jnp.zeros((seq_count,) + step_k.shape[1:], jnp.bfloat16), step_k, kv_place * step_dev, 0
    )
    own_v = lax.dynamic_update_slice_in_dim(
        jnp.zeros((seq_count,) + step_v.shape[1:], jnp.bfloat16), step_v, kv_place * step_dev, 0
    )
    head_scale = step_q.shape[-1] ** (-0.5)
    cache_scores = (
        jnp.einsum("bhcd,bkhcd->bhck", step_q, step_cache_keys, preferred_element_type=jnp.float32)
        * head_scale
    )
    fresh_scores = (
        jnp.einsum("bhcd,bhcd->bhc", step_q, own_k, preferred_element_type=jnp.float32) * head_scale
    )
    cache_place = kv_place * seq_cache + jnp.arange(seq_cache, dtype=jnp.int32)
    cache_visible = cache_place[None, :] < step_lens[:, None]
    cache_scores = jnp.where(cache_visible[:, None, None, :], cache_scores, -jnp.inf)
    fresh_scores = jnp.where(own_seq[:, None, None], fresh_scores, -jnp.inf)
    step_max = jnp.maximum(jnp.max(cache_scores, axis=-1), fresh_scores)
    cache_weights = jnp.exp(cache_scores - step_max[..., None])
    fresh_weights = jnp.exp(fresh_scores - step_max)
    step_tot = jnp.sum(cache_weights, axis=-1) + fresh_weights
    fresh_rounded = lax.optimization_barrier(fresh_weights.astype(jnp.bfloat16))
    step_acc = jnp.einsum(
        "bhck,bkhv->bhcv",
        cache_weights.astype(jnp.bfloat16),
        step_cache_values,
        preferred_element_type=jnp.float32,
    )
    step_acc = (
        step_acc
        + fresh_rounded.astype(jnp.float32)[..., None] * own_v.astype(jnp.float32)[:, :, None, :]
    )
    step_sum = lax.optimization_barrier(step_acc.astype(jnp.bfloat16))
    message = jnp.concatenate(
        [
            step_sum.astype(jnp.float32),
            step_max[..., None],
            step_tot[..., None],
            jnp.zeros(step_tot.shape + (126,), jnp.float32),
        ],
        axis=-1,
    ).reshape(kv_count, step_dev * parts, wide + 128)
    flat_heads = exchange(
        piece_sum,
        piece_stats,
        message,
        mix_ratio[None, :],
        out_gain[None, :],
        "kv",
        kv_count,
        maps,
        padded,
        1,
    )
    mixed = project_out(flat_heads, w_out.reshape(-1, w_out.shape[-1]), "tp", tp_count, 2)
    return (mixed[:piece_dev], mixed[piece_dev:end], piece_k, piece_v, step_k, step_v)


def solution(mesh):
    in_specs = (
        P("kv", None),
        P("kv", None),
        P(),
        P(None, "tp", None, None),
        P(None, "tp", None, None),
        P(None, "tp", None),
        P("tp", None, None),
        P("tp"),
        P(),
        P("kv", "tp", None, None),
        P("kv", "tp", None),
        P(None, "kv", "tp", None, None),
        P(None, "kv", "tp", None),
        P(),
        P(),
    )
    out_specs = (
        P("kv", "tp"),
        P("kv", "tp"),
        P("kv", "tp", None, None),
        P("kv", "tp", None),
        P("kv", "tp", None, None),
        P("kv", "tp", None),
    )
    return jax.shard_map(
        functools.partial(on_device, mesh.shape["kv"], mesh.shape["tp"]),
        mesh=mesh, in_specs=in_specs, out_specs=out_specs, check_vma=False
    )
```

profile of v0, /device:TPU:88, one launch (start us, length us, event | category | flops | bytes accessed | tf_op | source)
XLA Modules:
  0.0 265.5 jit_solution(11226101363333001135)
XLA Ops:
  2.1 0.6 iota_add_fusion.1.own_ref
  2.8 1.5 fusion.10
  4.4 0.7 broadcast_compare_fusion
  5.2 0.6 compare_select_fusion.bias_ref
  5.8 2.4 fusion.25
  8.3 0.6 slice.33
  8.8 0.6 slice_bitcast_fusion
  9.5 0.6 fusion.28
  10.2 0.5 copy.92
  10.7 0.6 slice_bitcast_fusion.1
  11.3 0.7 copy.60
  12.0 0.6 fusion.31
  12.6 0.6 copy.91
  13.3 1.1 copy.90
  14.4 53.8 %gather_rows.1.q_ref = bf16[32,112,256]{2,1,0:T(8,128)(2,1)} custom-call(bf16[112,256]{1,0:T(8,128)(2,1)} %bitcast.91), custom_call_target="tpu_custom_call" | custom-call | tf_op jit(solution)/shard_map/gather_rows/pallas_call | solution.py:62
  68.2 1.0 slice_reduce_fusion
  69.2 0.1 fusion.42
  69.3 0.1 copy.67
  69.4 2.8 %fusion.4 = f32[32,2,1,128]{3,2,1,0:T(1,128)S(1)} fusion(bf16[32,128,2,128]{3,2,1,0:T(2,128)(2,1)} %bitcast.85, bf16[32,112,256]{2,1,0:T(8,128)(2,1)} %gather_rows.1.q_ref), kind=kOutput, calls=%fused_computation.6 | convolution fusion | flops 2097152 | bytes 2162688 | tf_op jit(solution)/shard_map/bhcd,bkhcd->bhck/dot_general | solution.py:398
  72.2 0.1 fusion.50
  72.5 0.1 copy.56
  72.6 0.1 copy.55
  72.7 2.0 fusion.37
  74.7 0.2 fusion.44
  75.0 0.1 copy.59
  75.1 0.1 copy.58
  75.2 0.7 maximum_bitcast_fusion.step
  76.0 49.3 %attend.1 = (bf16[32,96,512]{2,1,0:T(8,128)(2,1)}, f32[32,96,128]{2,1,0:T(8,128)}) custom-call(bf16[32,112,256]{2,1,0:T(8,128)(2,1)} %gather_rows.1.q_ref, bf16[2,2048,128]{2,1,0:T(8,128)(2,1)} %bitcast.84, bf16[1,2048,256]{2,1,0:T(8,128)(2,1)} %bitcast.87, bf16[2,96,128]{2,1,0:T(8,128)(2,1)} %get-tuple-element.39.fk_ref, ...), custom_call_target="tpu_custom_call" | custom-call | tf_op jit(solution)/shard_map/attend/pallas_call | solution.py:117
  125.3 123.1 %exchange.1.heads = bf16[112,256]{1,0:T(8,128)(2,1)} custom-call(f32[1,1]{1,0:T(1,128)} %bitcast.81.ratio, f32[1,256]{1,0:T(1,128)} %bitcast.93, bf16[32,96,512]{2,1,0:T(8,128)(2,1)} %get-tuple-element.8.vals, f32[32,96,128]{2,1,0:T(8,128)} %get-tuple-element.9.stats, f32[32,2,384]{2,1,0:T(2,128)} %maximum_bitcast_fusion.step), custom_call_target="tpu_custom_call" | custom-call | tf_op jit(solution)/shard_map/exchange/pallas_call | solution.py:232
  248.4 14.3 %project_out.1 = bf16[112,512]{1,0:T(8,128)(2,1)} custom-call(bf16[112,256]{1,0:T(8,128)(2,1)} %exchange.1.heads, bf16[256,4096]{1,0:T(8,128)(2,1)} %bitcast.86), custom_call_target="tpu_custom_call" | custom-call | tf_op jit(solution)/shard_map/project_out/pallas_call | solution.py:305
  262.7 1.3 slice.29
  264.0 1.5 slice.28
  (33 shorter events, 0.5 us)
Async XLA Ops:
  0.6 2.1 copy-start
  5.8 3.7 %copy-start.2 = (bf16[96,4096]{1,0:T(8,128)(2,1)S(1)}, bf16[96,4096]{1,0:T(8,128)(2,1)}, u32[]{:S(2)}) copy-start(bf16[96,4096]{1,0:T(8,128)(2,1)} %param.15) | copy-start | bytes 2359300
  5.8 3.7 %copy-start.3 = (bf16[1,4096]{1,0:T(2,128)(2,1)S(1)}, bf16[1,4096]{1,0:T(2,128)(2,1)}, u32[]{:S(2)}) copy-start(bf16[1,4096]{1,0:T(2,128)(2,1)} %param.16) | copy-start | bytes 24580
  5.8 3.7 %copy-start.5 = (f32[4096]{0:T(1024)S(1)}, f32[4096]{0:T(1024)}, u32[]{:S(2)}) copy-start(f32[4096]{0:T(1024)} %param.17) | copy-start | bytes 49156
  9.5 2.5 copy-start.4
  12.0 1.3 copy-start.1
where the time goes:
time: 266 us; the launch traced here: 265 us
  Pallas kernels  240 us (90%)
  local copies, waits for them, and re-layouts  9.48 us (4%)
  matrix products  8.58 us (3%)
  other arithmetic  4.73 us (2%)
    pallas_call x1, Pallas kernels, exchange(): pl.pallas_call(functools.partial(exchange_kernel, axis, count, parts, map...  123 us
    pallas_call x1, Pallas kernels, gather_rows(): pl.pallas_call(functools.partial(gather_kernel, axis, count), out_shape=j...  53.8 us
    pallas_call x1, Pallas kernels, attend(): pl.pallas_call(functools.partial(attend_kernel, rows, dims), grid=(count...  49.3 us
    pallas_call x1, Pallas kernels, project_out(): pl.pallas_call(functools.partial(project_out_kernel, axis, count), out_sh...  14.3 us

commit v1 on v0

--- a/solution.py
+++ b/solution.py
@@ -73,74 +73,6 @@
     )(own)
 
 
-def attend_kernel(rows, dims, q_ref, k_ref, v_ref, fk_ref, fv_ref, bias_ref, own_ref, o_ref, s_ref):
-    part = pl.program_id(1)
-    owners = q_ref.shape[0]
-    scale = dims ** (-0.5)
-    fold = scale * math.log2(math.e)
-    q = q_ref[:, :rows, :].reshape(owners * rows, dims)
-    contract = (((1,), (1,)), ((), ()))
-    old = lax.dot_general(q, k_ref[0], contract, preferred_element_type=jnp.float32)
-    old = old + bias_ref[...]
-    new = lax.dot_general(q, fk_ref[0], contract, preferred_element_type=jnp.float32)
-    place = pl.program_id(0) * owners * rows + lax.broadcasted_iota(jnp.int32, new.shape, 0)
-    new = jnp.where(own_ref[...] <= place, new, HIDDEN)
-    top = jnp.maximum(
-        jnp.max(old, axis=1, keepdims=True), jnp.max(new, axis=1, keepdims=True)
-    )
-    old_w = jnp.exp2((old - top) * fold)
-    new_w = jnp.exp2((new - top) * fold)
-    total = jnp.sum(old_w, axis=1, keepdims=True) + jnp.sum(new_w, axis=1, keepdims=True)
-    summed = jnp.dot(old_w.astype(jnp.bfloat16), v_ref[0], preferred_element_type=jnp.float32)
-    summed += jnp.dot(new_w.astype(jnp.bfloat16), fv_ref[0], preferred_element_type=jnp.float32)
-    o_ref[...] = summed.astype(jnp.bfloat16).reshape(o_ref.shape)
-    parts = pl.num_programs(1)
-    lane = lax.broadcasted_iota(jnp.int32, (owners * rows, s_ref.shape[-1]), 1)
-    put = jnp.where(lane == part, top * scale, jnp.where(lane == parts + part, total, 0.0))
-    put = put.reshape(s_ref.shape)
-
-    @pl.when(part == 0)
-    def _():
-        s_ref[...] = put
-
-    @pl.when(part != 0)
-    def _():
-        s_ref[...] += put
-
-
-def attend(q_all, keys, values, fresh_k, fresh_v, bias, fresh_place, rows):
-    count, padded, _ = q_all.shape
-    parts, cached, dims = keys.shape
-    maps = parts // values.shape[0]
-    wide = values.shape[-1]
-    owners = math.gcd(count, 2)
-    return pl.pallas_call(
-        functools.partial(attend_kernel, rows, dims),
-        grid=(count // owners, parts),
-        in_specs=[
-            pl.BlockSpec((owners, padded, dims), lambda i, p: (i, 0, p)),
-            pl.BlockSpec((1, cached, dims), lambda i, p: (p, 0, 0)),
-            pl.BlockSpec((1, cached, wide), lambda i, p: (p // maps, 0, 0)),
-            pl.BlockSpec((1, rows, dims), lambda i, p: (p, 0, 0)),
-            pl.BlockSpec((1, rows, wide), lambda i, p: (p // maps, 0, 0)),
-            pl.BlockSpec((1, cached), lambda i, p: (0, 0)),
-            pl.BlockSpec((1, rows), lambda i, p: (0, 0)),
-        ],
-        out_specs=[
-            pl.BlockSpec((owners, rows, wide), lambda i, p: (i, 0, p)),
-            pl.BlockSpec((owners, rows, 128), lambda i, p: (i, 0, 0)),
-        ],
-        out_shape=[
-            jax.ShapeDtypeStruct((count, rows, parts * wide), jnp.bfloat16),
-            jax.ShapeDtypeStruct((count, rows, 128), jnp.float32),
-        ],
-        compiler_params=pltpu.CompilerParams(
-            dimension_semantics=("arbitrary", "arbitrary"), vmem_limit_bytes=56 * 1024 * 1024
-        ),
-        name="attend",
-    )(q_all, keys, values, fresh_k, fresh_v, bias, fresh_place)
-
-
 def mix_maps(first, second, ratio, gain):
     mixed = first - ratio * second
     inv_rms = lax.rsqrt(jnp.mean(mixed * mixed, axis=-1, keepdims=True) + EPS)
@@ -156,96 +88,323 @@
     return total / norm
 
 
-def exchange_kernel(
-    axis, count, parts, maps, wide, ratio, gain, vals, stats, step, out, all_v, all_s, all_t, send_sem, recv_sem
+SIDE_Y = 4
+TILE = 128
+
+
+def spread(stats, first, groups, width):
+    cols = [jnp.broadcast_to(stats[:, i : i + 1], (8, width)) for i in range(first, first + groups)]
+    return jnp.concatenate(cols, axis=0)
+
+
+def pack_columns(columns):
+    lane = lax.broadcasted_iota(jnp.int32, (8, TILE), 1)
+    out = jnp.zeros((8, TILE), jnp.float32)
+    for place, column in columns:
+        out = jnp.where(lane == place, column, out)
+    return out
+
+
+def ring_kernel(
+    kv_count, fold, ratio, gain, q_own, kt, values, bias, step, out,
+    q_all, scores, weights, sent_v, sent_s, got_v, got_s, far_v, far_s, all_t,
+    qz_send, qz_recv, qy_send, qy_recv, r_send, r_recv, f_send, f_recv, t_send, t_recv,
 ):
-    me = meet(axis, count)
-    copies = []
-    for turn in range(1, count):
-        other = lax.rem(me + turn, count)
-        for slot, (mine, theirs) in enumerate(((stats, all_s), (step, all_t), (vals, all_v))):
-            copy = pltpu.make_async_remote_copy(
-                src_ref=mine.at[other],
-                dst_ref=theirs.at[me],
-                send_sem=send_sem.at[turn, slot],
-                recv_sem=recv_sem.at[turn, slot],
-                device_id={axis: other},
-                device_id_type=MESH,
+    ny = SIDE_Y
+    nz = kv_count // ny
+    rows, dims = q_own.shape[1:]
+    wide = values.shape[1]
+    cached = bias.shape[1]
+    total_keys = values.shape[0]
+    half = 2 * rows
+    blocks = rows // 8
+    me = lax.axis_index("kv")
+    z = me // ny
+    y = lax.rem(me, ny)
+    other_z = [lax.rem(z + 1, nz) * ny + y, lax.rem(z + nz - 1, nz) * ny + y]
+
+    def to(src, dst, send, recv, device):
+        return pltpu.make_async_remote_copy(
+            src_ref=src, dst_ref=dst, send_sem=send, recv_sem=recv,
+            device_id={"kv": device}, device_id_type=MESH,
+        )
+
+    def along_z(m, slot, source):
+        return to(source, q_all.at[m, slot, y], qz_send.at[m, slot], qz_recv.at[m, slot], other_z[m])
+
+    def along_y(m, slot, turn, source):
+        return to(
+            source, q_all.at[m, slot, y], qy_send.at[m, slot, turn], qy_recv.at[m, slot, y],
+            z * ny + lax.rem(y + turn, ny),
+        )
+
+    def from_y(m, slot, turn):
+        there = lax.rem(y + turn, ny)
+        return to(
+            q_all.at[m, slot, there], q_all.at[m, slot, there],
+            qy_send.at[m, slot, turn], qy_recv.at[m, slot, there], z * ny + there,
+        )
+
+    def ring(m, slot, h):
+        at = pl.ds(h * half, half)
+        return (
+            to(sent_s.at[m, slot, h], got_s.at[m, slot + 1, h],
+               r_send.at[m, slot, h, 0], r_recv.at[m, slot, h, 0], other_z[m]),
+            to(sent_v.at[m, slot, at], got_v.at[m, slot + 1, at],
+               r_send.at[m, slot, h, 1], r_recv.at[m, slot, h, 1], other_z[m]),
+        )
+
+    def final(m, there):
+        at = pl.ds(pl.multiple_of(there * rows, 32), rows)
+        return (
+            to(sent_s.at[m, nz - 1, there // 2], far_s.at[m, y],
+               f_send.at[m, there, 0], f_recv.at[m, y, 0], z * ny + there),
+            to(sent_v.at[m, nz - 1, at], far_v.at[m, y],
+               f_send.at[m, there, 1], f_recv.at[m, y, 1], z * ny + there),
+        )
+
+    def final_from(m, there):
+        return (
+            to(far_s.at[m, there], far_s.at[m, there],
+               f_send.at[m, there, 0], f_recv.at[m, there, 0], z * ny + there),
+            to(far_v.at[m, there], far_v.at[m, there],
+               f_send.at[m, there, 1], f_recv.at[m, there, 1], z * ny + there),
+        )
+
+    meet("kv", kv_count)
+    for m in range(2):
+        along_z(m, 0, q_own.at[m]).start()
+    for m in range(2):
+        for turn in range(1, ny):
+            along_y(m, nz - 1, turn, q_own.at[m]).start()
+    step_copies = []
+    for turn in range(1, kv_count):
+        there = lax.rem(me + turn, kv_count)
+        copy = to(step.at[there], all_t.at[me], t_send.at[turn], t_recv.at[turn], there)
+        copy.start()
+        step_copies.append(copy)
+    all_t[me] = step[me]
+    for m in range(2):
+        q_all[m, nz - 1, y] = q_own[m]
+        got_v[m, 0] = jnp.zeros(got_v.shape[2:], jnp.bfloat16)
+        lane = lax.broadcasted_iota(jnp.int32, (8, TILE), 1)
+        tops = lax.rem(lane, 2 * blocks) < blocks
+        for h in range(2):
+            got_s[m, 0, h] = jnp.where(tops, HIDDEN, 0.0)
+
+    def pass_on(slot):
+        for m in range(2):
+            along_z(m, slot, q_own.at[m]).wait_recv()
+
+            @pl.when(slot < nz - 2)
+            def _():
+                along_z(m, slot + 1, q_all.at[m, slot, y]).start()
+
+            for turn in range(1, ny):
+                along_y(m, slot, turn, q_all.at[m, slot, y]).start()
+
+    pass_on(0)
+
+    def score(m, h, slot, off):
+        q = q_all[m, slot, 2 * h : 2 * h + 2].reshape(half, dims)
+        buf = (2 * m + h) % 2
+        best = None
+        for c in range(0, cached, 256):
+            s = jnp.dot(q, kt[m, :, c : c + 256], preferred_element_type=jnp.float32)
+            s = s + bias[:, c : c + 256]
+            scores[buf, :, c : c + 256] = s
+            for j in range(0, 256, TILE):
+                p = s[:, j : j + TILE]
+                best = p if best is None else jnp.maximum(best, p)
+        tail = jnp.dot(q, kt[m, :, cached:], preferred_element_type=jnp.float32)
+        lane = lax.broadcasted_iota(jnp.int32, tail.shape, 1)
+        row = lax.broadcasted_iota(jnp.int32, tail.shape, 0)
+        gap = jnp.where(lane < rows, lane - row, 1 << 20)
+        tail = jnp.where(gap <= off, tail, HIDDEN)
+        scores[buf, :, cached:] = tail
+        best = jnp.maximum(best, tail)
+        return jnp.max(best, axis=1, keepdims=True)
+
+    def weigh(m, h, top):
+        buf = (2 * m + h) % 2
+        part = None
+        for c in range(0, total_keys, TILE):
+            w = jnp.exp2((scores[buf, :, c : c + TILE] - top) * fold)
+            weights[buf, :, c : c + TILE] = w.astype(jnp.bfloat16)
+            part = w if part is None else part + w
+        total = jnp.sum(part, axis=1, keepdims=True)
+        return jnp.dot(weights[buf], values[...], preferred_element_type=jnp.float32), total
+
+    def join(m, h, slot, top, total, summed):
+        at = pl.ds(h * half, half)
+        old = got_s[m, slot, h]
+        old_top = jnp.concatenate([spread(old, 2 * blocks * j, blocks, TILE) for j in range(2)], axis=0)
+        old_total = jnp.concatenate(
+            [spread(old, 2 * blocks * j + blocks, blocks, TILE) for j in range(2)], axis=0
+        )
+        best = jnp.maximum(old_top, top)
+        old_scale = jnp.exp2((old_top - best) * fold)
+        new_scale = jnp.exp2((top - best) * fold)
+        norm = old_total * old_scale + total * new_scale
+        for c in range(0, wide, TILE):
+            mixed = got_v[m, slot, at, c : c + TILE].astype(jnp.float32) * old_scale
+            mixed = mixed + summed[:, c : c + TILE] * new_scale
+            sent_v[m, slot, at, c : c + TILE] = mixed.astype(jnp.bfloat16)
+        columns = []
+        for j in range(2):
+            for i in range(blocks):
+                line = slice(j * rows + i * 8, j * rows + i * 8 + 8)
+                columns.append((2 * blocks * j + i, best[line]))
+                columns.append((2 * blocks * j + blocks + i, norm[line]))
+        sent_s[m, slot, h] = pack_columns(columns)
+
+    units = [(m, h) for m in range(2) for h in range(2)]
+
+    def turn_step(slot, carry):
+        @pl.when(slot < nz - 2)
+        def _():
+            pass_on(slot + 1)
+
+        for m in range(2):
+            for turn in range(1, ny):
+                from_y(m, slot, turn).wait_recv()
+        homes = [lax.rem(z + nz - 1 - slot, nz), lax.rem(z + 1 + slot, nz)]
+        offs = [[(homes[m] * ny + 2 * h - me) * rows for h in range(2)] for m in range(2)]
+        tops = [None] * len(units)
+        tops[0] = score(0, 0, slot, offs[0][0])
+        for u, (m, h) in enumerate(units):
+            if u + 1 < len(units):
+                m2, h2 = units[u + 1]
+                tops[u + 1] = score(m2, h2, slot, offs[m2][h2])
+            summed, total = weigh(m, h, tops[u])
+
+            @pl.when(slot > 0)
+            def _():
+                for copy in ring(m, slot - 1, h):
+                    copy.wait_recv()
+
+            join(m, h, slot, tops[u], total, summed)
+
+            @pl.when(slot < nz - 1)
+            def _():
+                for copy in ring(m, slot, h):
+                    copy.start()
+
+            @pl.when(slot == nz - 1)
+            def _():
+                for there in range(2 * h, 2 * h + 2):
+                    @pl.when(y != there)
+                    def _():
+                        for copy in final(m, there):
+                            copy.start()
+        return carry
+
+    lax.fori_loop(0, nz, turn_step, 0)
+
+    for copy in step_copies:
+        copy.wait()
+    low = out.shape[0] - rows
+    maps_out = []
+    for m in range(2):
+        maps_out.append(
+            blend(
+                [all_t[g, m : m + 1, :wide] for g in range(kv_count)],
+                [all_t[g, m : m + 1, wide : wide + 1] for g in range(kv_count)],
+                [all_t[g, m : m + 1, wide + 1 : wide + 2] for g in range(kv_count)],
             )
-            copy.start()
-            copies.append(copy)
-    all_v[me] = vals[me]
-    all_s[me] = stats[me]
-    all_t[me] = step[me]
-    for copy in copies:
-        copy.wait()
-    rows = vals.shape[1]
-    steps = step.shape[1] // parts
-    out[...] = jnp.zeros_like(out)
-    tall = math.gcd(rows, 32)
-
-    def chunk(index, carry):
-        at = pl.ds(pl.multiple_of(index * tall, tall), tall)
-        for head in range(parts // maps):
-            maps_out = []
-            for part in range(head * maps, head * maps + maps):
-                cut = slice(part * wide, part * wide + wide)
-                maps_out.append(
-                    blend(
-                        [all_v[g, at, cut].astype(jnp.float32) for g in range(count)],
-                        [all_s[g, at, part : part + 1] for g in range(count)],
-                        [all_s[g, at, parts + part : parts + part + 1] for g in range(count)],
-                    )
-                )
-            out[at, head * wide : head * wide + wide] = mix_maps(
-                maps_out[0], maps_out[1], ratio[0, head], gain[...]
-            )
+        )
+    line = mix_maps(maps_out[0], maps_out[1], ratio[0, 0], gain[...]).astype(jnp.float32)
+    place = lax.broadcasted_iota(jnp.int32, (low, wide), 0)
+    out[rows:, :] = jnp.where(place == 0, line, 0.0).astype(jnp.bfloat16)
+
+    for m in range(2):
+        for turn in range(1, ny):
+            for copy in final_from(m, lax.rem(y + turn, ny)):
+                copy.wait_recv()
+    odd = lax.rem(y, 2) == 1
+
+    def own_half(stats):
+        return jnp.where(odd, pltpu.roll(stats, TILE - 2 * blocks, 1), stats)
+
+    stats = [
+        [own_half(sent_s[m, nz - 1, y // 2])]
+        + [own_half(far_s[m, lax.rem(y + turn, ny)]) for turn in range(1, ny)]
+        for m in range(2)
+    ]
+    tall = 32
+    for j in range(rows // tall):
+        maps_out = []
+        for m in range(2):
+            at = pl.ds(pl.multiple_of(y * rows + j * tall, tall), tall)
+            vals = [sent_v[m, nz - 1, at, :]]
+            vals += [far_v[m, lax.rem(y + turn, ny), j * tall : (j + 1) * tall, :] for turn in range(1, ny)]
+            tops = [spread(s, j * tall // 8, tall // 8, wide) for s in stats[m]]
+            totals = [spread(s, blocks + j * tall // 8, tall // 8, wide) for s in stats[m]]
+            best = functools.reduce(jnp.maximum, tops)
+            scales = [jnp.exp2((t - best) * fold) for t in tops]
+            norm = functools.reduce(jnp.add, [a * b for a, b in zip(scales, totals)])
+            total = functools.reduce(jnp.add, [a * b.astype(jnp.float32) for a, b in zip(scales, vals)])
+            maps_out.append(total / norm)
+        out[j * tall : (j + 1) * tall, :] = mix_maps(maps_out[0], maps_out[1], ratio[0, 0], gain[...])
+
+    for m in range(2):
+        for there in range(ny):
+            @pl.when(y != there)
+            def _():
+                for copy in final(m, there):
+                    copy.wait_send()
+        for turn in range(1, ny):
+            along_y(m, nz - 1, turn, q_own.at[m]).wait_send()
+
+    def drain(slot, carry):
+        for m in range(2):
+            along_z(m, slot, q_own.at[m]).wait_send()
+            for turn in range(1, ny):
+                along_y(m, slot, turn, q_own.at[m]).wait_send()
+            for h in range(2):
+                for copy in ring(m, slot, h):
+                    copy.wait_send()
         return carry
 
-    lax.fori_loop(0, rows // tall, chunk, 0)
-    low = out.shape[0] - rows
-    for head in range(parts // maps):
-        lines = []
-        for seq in range(steps):
-            maps_out = []
-            for part in range(seq * parts + head * maps, seq * parts + head * maps + maps):
-                line = [all_t[g, part : part + 1, :] for g in range(count)]
-                maps_out.append(
-                    blend(
-                        [v[:, :wide] for v in line],
-                        [v[:, wide : wide + 1] for v in line],
-                        [v[:, wide + 1 : wide + 2] for v in line],
-                    )
-                )
-            lines.append(mix_maps(maps_out[0], maps_out[1], ratio[0, head], gain[...]).astype(jnp.float32))
-        place = lax.broadcasted_iota(jnp.int32, (low, wide), 0)
-        block = jnp.zeros((low, wide), jnp.float32)
-        for seq in range(steps):
-            block = jnp.where(place == seq, lines[seq], block)
-        out[rows:, head * wide : head * wide + wide] = block.astype(jnp.bfloat16)
-
-
-def exchange(values, stats, step, ratio, gain, axis, count, maps, padded, collective):
-    parts = values.shape[-1] // gain.shape[-1]
-    wide = gain.shape[-1]
+    lax.fori_loop(0, nz - 1, drain, 0)
+
+
+def ring_attend(q_own, kt, values, bias, step, ratio, gain, kv_count, padded, collective):
+    rows, dims = q_own.shape[1:]
+    wide = values.shape[1]
+    keys = values.shape[0]
+    ny = SIDE_Y
+    nz = kv_count // ny
     vmem = pl.BlockSpec(memory_space=pltpu.VMEM)
+    dma = pltpu.SemaphoreType.DMA
+    fold = dims ** (-0.5) * math.log2(math.e)
     return pl.pallas_call(
-        functools.partial(exchange_kernel, axis, count, parts, maps, wide),
-        out_shape=jax.ShapeDtypeStruct((padded, parts // maps * wide), jnp.bfloat16),
-        in_specs=[pl.BlockSpec(memory_space=pltpu.SMEM), vmem, vmem, vmem, vmem],
+        functools.partial(ring_kernel, kv_count, fold),
+        out_shape=jax.ShapeDtypeStruct((padded, wide), jnp.bfloat16),
+        in_specs=[pl.BlockSpec(memory_space=pltpu.SMEM)] + [vmem] * 6,
         out_specs=vmem,
         scratch_shapes=[
-            pltpu.VMEM(values.shape, values.dtype),
-            pltpu.VMEM(stats.shape, stats.dtype),
+            pltpu.VMEM((2, nz, ny, rows, dims), jnp.bfloat16),
+            pltpu.VMEM((2, 2 * rows, keys), jnp.float32),
+            pltpu.VMEM((2, 2 * rows, keys), jnp.bfloat16),
+            pltpu.VMEM((2, nz, ny * rows, wide), jnp.bfloat16),
+            pltpu.VMEM((2, nz, 2, 8, TILE), jnp.float32),
+            pltpu.VMEM((2, nz, ny * rows, wide), jnp.bfloat16),
+            pltpu.VMEM((2, nz, 2, 8, TILE), jnp.float32),
+            pltpu.VMEM((2, ny, rows, wide), jnp.bfloat16),
+            pltpu.VMEM((2, ny, 8, TILE), jnp.float32),
             pltpu.VMEM(step.shape, step.dtype),
-            pltpu.SemaphoreType.DMA((count, 3)),
-            pltpu.SemaphoreType.DMA((count, 3)),
+            dma((2, nz)), dma((2, nz)),
+            dma((2, nz, ny)), dma((2, nz, ny)),
+            dma((2, nz, 2, 2)), dma((2, nz, 2, 2)),
+            dma((2, ny, 2)), dma((2, ny, 2)),
+            dma((kv_count,)), dma((kv_count,)),
         ],
         compiler_params=pltpu.CompilerParams(
             collective_id=collective, has_side_effects=True, vmem_limit_bytes=56 * 1024 * 1024
         ),
-        name="exchange",
-    )(ratio, gain, values, stats, step)
+        name="ring_attend",
+    )(ratio, gain, q_own, kt, values, bias, step)
 
 
 def project_out_kernel(axis, count, heads, weight, out, terms, pair, half, far, d_send, d_recv, x_send, x_recv):
@@ -359,8 +518,8 @@
     queries = project(normed, w_query)
     key_rows = project(normed, w_key)
     value_rows = project(normed, w_value)
-    q_flat = jnp.transpose(queries, (1, 0, 2)).reshape(padded, parts * dims)
-    q_all = gather_rows(q_flat, "kv", kv_count, 0)
+    step_flat = queries[:, piece_dev].astype(jnp.float32)
+    q_all = gather_rows(step_flat, "kv", kv_count, 0)
     end = piece_dev + step_dev
 
     def rows_of(flat, start, stop, extra):
@@ -370,22 +529,16 @@
     step_k = rows_of(key_rows, piece_dev, end, (heads, maps, dims))
     piece_v = rows_of(value_rows, 0, piece_dev, (heads, wide))
     step_v = rows_of(value_rows, piece_dev, end, (heads, wide))
-    keys = jnp.transpose(prompt_keys, (1, 2, 0, 3)).reshape(parts, cache_dev, dims)
-    values = jnp.transpose(prompt_values, (1, 0, 2))
+    spare_keys = -(-piece_dev // TILE) * TILE - piece_dev
+    keys = jnp.transpose(prompt_keys, (1, 2, 3, 0)).reshape(parts, dims, cache_dev)
+    fresh_k = jnp.transpose(key_rows[:, :piece_dev], (0, 2, 1))
+    kt = jnp.concatenate([keys, fresh_k, jnp.zeros((parts, dims, spare_keys), jnp.bfloat16)], axis=2)
+    all_v = jnp.concatenate(
+        [prompt_values[:, 0], value_rows[0, :piece_dev], jnp.zeros((spare_keys, wide), jnp.bfloat16)], axis=0
+    )
     cache_ok = kv_place * cache_dev + jnp.arange(cache_dev, dtype=jnp.int32) < prompt_len[0]
     bias = jnp.where(cache_ok, 0.0, HIDDEN)[None, :]
-    fresh_place = (kv_place * piece_dev + jnp.arange(piece_dev, dtype=jnp.int32))[None, :]
-    piece_sum, piece_stats = attend(
-        q_all,
-        keys,
-        values,
-        key_rows[:, :piece_dev],
-        value_rows[:, :piece_dev],
-        bias,
-        fresh_place,
-        piece_dev,
-    )
-    step_q = q_all[:, piece_dev:end].reshape(seq_count, heads, maps, dims)
+    step_q = q_all.astype(jnp.bfloat16).reshape(seq_count, heads, maps, dims)
     own_seq = jnp.arange(seq_count, dtype=jnp.int32) // step_dev == kv_place
     own_k = lax.dynamic_update_slice_in_dim(
         jnp.zeros((seq_count,) + step_k.shape[1:], jnp.bfloat16), step_k, kv_place * step_dev, 0
@@ -430,17 +583,8 @@
         ],
         axis=-1,
     ).reshape(kv_count, step_dev * parts, wide + 128)
-    flat_heads = exchange(
-        piece_sum,
-        piece_stats,
-        message,
-        mix_ratio[None, :],
-        out_gain[None, :],
-        "kv",
-        kv_count,
-        maps,
-        padded,
-        1,
+    flat_heads = ring_attend(
+        queries[:, :piece_dev], kt, all_v, bias, message, mix_ratio[None, :], out_gain[None, :], kv_count, padded, 1
     )
     mixed = project_out(flat_heads, w_out.reshape(-1, w_out.shape[-1]), "tp", tp_count, 2)
     return (mixed[:piece_dev], mixed[piece_dev:end], piece_k, piece_v, step_k, step_v)

time: 266 us -> 129 us (0.48)
  the two profiles are of different devices: /device:TPU:88 before, /device:TPU:1 now
where the time goes in v1:
time: 129 us
  Pallas kernels  98.4 us (76%)
  local copies, waits for them, and re-layouts  11 us (9%)
  matrix products  10.1 us (8%)
  other arithmetic  7.06 us (5%)
  between operations  2.29 us (2%)
    pallas_call x1, Pallas kernels, ring_attend(): pl.pallas_call(functools.partial(ring_kernel, kv_count, fold), out_shape=...  62.2 us
    pallas_call x1, Pallas kernels, project_out(): pl.pallas_call(functools.partial(project_out_kernel, axis, count), out_sh...  20.3 us
    pallas_call x1, Pallas kernels, gather_rows(): pl.pallas_call(functools.partial(gather_kernel, axis, count), out_shape=j...  15.9 us
    dot_general x3, matrix products, project(): jnp.einsum('nd,gdk->gnk', normed, parts, preferred_element_type=jnp.float32)  5.29 us
    unnamed x14, local copies, waits for them, and re-layouts  3.34 us
    dot_general x1, matrix products, on_device(): jnp.einsum('bhcd,bkhcd->bhck', step_q, step_cache_keys, preferred_element...  2.76 us

profile of v1, /device:TPU:1, one launch (start us, length us, event | category | flops | bytes accessed | tf_op | source)
XLA Modules:
  0.0 128.8 jit_solution(16124876989704000796)
XLA Ops:
  2.1 0.1 copy-done
  2.3 1.5 %fusion.10 = f32[112]{0:T(128)S(1)} fusion(bf16[1,4096]{1,0:T(2,128)(2,1)} %param.16, bf16[96,4096]{1,0:T(8,128)(2,1)} %param.15, bf16[112]{0:T(256)(128)(2,1)S(1)} %pad.9.clone), kind=kLoop, calls=%fused_computation.12 | loop fusion | flops 3669904 | bytes 795296 | tf_op jit(solution)/shard_map/reduce_sum | solution.py:19
  4.0 0.7 broadcast_compare_fusion
  4.7 0.6 compare_select_fusion.bias
  5.3 2.4 %fusion.25 = bf16[1,112,256]{2,1,0:T(8,128)(2,1)S(1)} fusion(bf16[4096,1,256]{2,0,1:T(8,128)(2,1)} %param.20, f32[4096]{0:T(1024)} %param.17, f32[112]{0:T(128)S(1)} %add_rsqrt_fusion, bf16[1,4096]{1,0:T(2,128)(2,1)} %param.16, bf16[96,4096]{1,0:T(8,128)(2,1)} %param.15, bf16[112]{0:T(256)(128)(2,1)S(1)} %pad.9.clone), kind=kOutput, calls=%fused_computation.19 | convolution fusion | flops 239038464 | bytes 2966176 | tf_op jit(solution)/shard_map/nd,gdk->gnk/dot_general | solution.py:27
  7.8 0.6 slice.39
  8.4 0.6 slice_bitcast_fusion.2
  9.0 0.6 fusion.28
  9.7 0.6 slice_convert_fusion
  10.2 0.6 slice.34.q_own
  10.8 15.9 %gather_rows.1 = f32[32,2,128]{2,1,0:T(2,128)} custom-call(f32[2,128]{1,0:T(2,128)} %bitcast.89), custom_call_target="tpu_custom_call" | custom-call | tf_op jit(solution)/shard_map/gather_rows/pallas_call | solution.py:62
  26.8 2.2 %fusion.16 = bf16[112,2,128]{2,0,1:T(8,128)(2,1)S(1)} fusion(bf16[2,4096,128]{2,0,1:T(2,128)(2,1)} %bitcast.92, f32[4096]{0:T(1024)S(1)} %copy-done.5, f32[112]{0:T(128)S(1)} %add_rsqrt_fusion, bf16[1,4096]{1,0:T(2,128)(2,1)S(1)} %copy-done.3, bf16[96,4096]{1,0:T(8,128)(2,1)S(1)} %copy-done.1, bf16[112]{0:T(256)(128)(2,1)S(1)} %pad.9.clone), kind=kOutput, calls=%fused_computation.16 | convolution fusion | flops 239038464 | bytes 2966176 | tf_op jit(solution)/shard_map/nd,gdk->gnk/dot_general | solution.py:27
  29.0 0.1 copy.53
  29.2 0.2 slice_reduce_fusion
  29.4 0.1 convert_bitcast_fusion
  29.6 2.8 %fusion.4 = f32[32,2,1,128]{3,2,1,0:T(1,128)S(1)} fusion(bf16[32,128,2,128]{3,2,1,0:T(2,128)(2,1)} %bitcast.93, bf16[32,2,128,1]{2,1,0,3:T(2,128)(2,1)S(1)} %get-tuple-element.36), kind=kOutput, calls=%fused_computation.6 | convolution fusion | flops 2097152 | bytes 2146304 | tf_op jit(solution)/shard_map/bhcd,bkhcd->bhck/dot_general | solution.py:551
  32.4 0.1 fusion.46
  32.6 0.1 copy.56
  32.7 0.1 copy.55
  32.8 2.0 %fusion.34 = bf16[32,1,2,256]{3,2,0,1:T(2,128)(2,1)S(1)} fusion(bf16[32,128,1,256]{3,1,2,0:T(8,128)(2,1)} %param.27, f32[32,256]{1,0:T(8,128)S(1)} %mul.76, f32[32,2]{1,0:T(8,128)S(1)} %copy.56, f32[32,2]{1,0:T(8,128)S(1)} %copy.55, f32[32,2,128]{2,1,0:T(2,128)S(1)} %bitcast.86, pred[32,128]{1,0:T(8,128)(4,1)S(1)} %broadcast_compare_fusion), kind=kOutput, calls=%fused_computation.23 | convolution fusion | flops 4276224 | bytes 2200064 | tf_op jit(solution)/shard_map/bhck,bkhv->bhcv/dot_general | solution.py:566
  34.8 0.2 fusion.41
  35.1 0.1 copy.59
  35.3 0.1 copy.58
  35.4 0.7 maximum_bitcast_fusion.step
  36.1 0.7 copy.60
  36.9 2.4 %copy.51 = bf16[2048,1,2,128]{0,3,2,1:T(8,128)(2,1)S(1)} copy(bf16[2048,1,2,128]{3,2,1,0:T(2,128)(2,1)} %param.24) | data formatting | bytes 2097152 | tf_op args[9]
  39.4 1.8 %concatenate.13.kt = bf16[2,128,2176]{2,1,0:T(8,128)(2,1)} concatenate(bf16[2,128,2048]{2,1,0:T(8,128)(2,1)S(1)} %bitcast.80, bf16[2,128,96]{2,1,0:T(8,128)(2,1)S(1)} %get-tuple-element.33, bf16[2,128,32]{2,1,0:T(8,128)(2,1)S(1)} %broadcast_in_dim.71), dimensions={2} | concatenate | bytes 2228224 | tf_op jit(solution)/shard_map/concatenate | solution.py:535
  41.2 2.3 %pad_maximum_fusion.values = bf16[2176,256]{1,0:T(8,128)(2,1)} fusion(bf16[32,256]{1,0:T(8,128)(2,1)S(1)} %broadcast_in_dim.72, bf16[96,256]{1,0:T(8,128)(2,1)S(1)} %get-tuple-element.35, bf16[2048,256]{1,0:T(8,128)(2,1)} %bitcast.82), kind=kLoop, calls=%fused_computation.22 | loop fusion | flops 3342336 | bytes 2228224 | tf_op jit(solution)/shard_map/concatenate | solution.py:536
  43.5 62.2 %ring_attend.1.heads = bf16[112,256]{1,0:T(8,128)(2,1)} custom-call(f32[1,1]{1,0:T(1,128)} %bitcast.77.ratio, f32[1,256]{1,0:T(1,128)} %bitcast.90, bf16[2,96,128]{2,1,0:T(8,128)(2,1)} %slice.34.q_own, bf16[2,128,2176]{2,1,0:T(8,128)(2,1)} %concatenate.13.kt, bf16[2176,256]{1,0:T(8,128)(2,1)} %pad_maximum_fusion.values, f32[1,2048]{1,0:T(1,128)} %compare_select_fusion.bias, ...), custom_call_target="tpu_custom_call" | custom-call | tf_op jit(solution)/shard_map/ring_attend/pallas_call | solution.py:381
  105.7 20.3 %project_out.1 = bf16[112,512]{1,0:T(8,128)(2,1)} custom-call(bf16[112,256]{1,0:T(8,128)(2,1)} %ring_attend.1.heads, bf16[256,4096]{1,0:T(8,128)(2,1)} %bitcast.81), custom_call_target="tpu_custom_call" | custom-call | tf_op jit(solution)/shard_map/project_out/pallas_call | solution.py:464
  126.0 1.3 slice.33
  127.3 1.5 %slice.32 = bf16[96,512]{1,0:T(8,128)(2,1)} slice(bf16[112,512]{1,0:T(8,128)(2,1)} %project_out.1), slice={[0:96], [0:512]} | slice | bytes 196608 | tf_op jit(solution)/shard_map/slice | solution.py:590
  (34 shorter events, 0.6 us)
Async XLA Ops:
  0.6 1.6 %copy-start = (bf16[4096,1,2,128]{3,2,1,0:T(2,128)(2,1)S(1)}, bf16[4096,1,2,128]{3,2,1,0:T(2,128)(2,1)}, u32[]{:S(2)}) copy-start(bf16[4096,1,2,128]{3,2,1,0:T(2,128)(2,1)} %param.18) | copy-start | bytes 6291460
  5.3 3.7 %copy-start.1 = (bf16[96,4096]{1,0:T(8,128)(2,1)S(1)}, bf16[96,4096]{1,0:T(8,128)(2,1)}, u32[]{:S(2)}) copy-start(bf16[96,4096]{1,0:T(8,128)(2,1)} %param.15) | copy-start | bytes 2359300
  5.3 3.7 %copy-start.3 = (bf16[1,4096]{1,0:T(2,128)(2,1)S(1)}, bf16[1,4096]{1,0:T(2,128)(2,1)}, u32[]{:S(2)}) copy-start(bf16[1,4096]{1,0:T(2,128)(2,1)} %param.16) | copy-start | bytes 24580
  5.3 3.7 %copy-start.5 = (f32[4096]{0:T(1024)S(1)}, f32[4096]{0:T(1024)}, u32[]{:S(2)}) copy-start(f32[4096]{0:T(1024)} %param.17) | copy-start | bytes 49156
  26.8 2.6 %copy-start.2 = (f32[32,2,128]{2,1,0:T(2,128)S(1)}, f32[32,2,128]{2,1,0:T(2,128)}, u32[]{:S(2)}) copy-start(f32[32,2,128]{2,1,0:T(2,128)} %gather_rows.1) | copy-start | bytes 98308
  29.4 5.5 %copy-start.4 = (bf16[2,128]{1,0:T(2,128)(2,1)}, bf16[2,128]{1,0:T(2,128)(2,1)S(1)}, u32[]{:S(2)}) copy-start(bf16[2,128]{1,0:T(2,128)(2,1)S(1)} %slice_reduce_fusion) | copy-start | bytes 1540

commit v2 on v1

v2 whole, which is shorter than its diff:
```python
import functools
import math

import jax
import jax.numpy as jnp
from jax import lax
from jax.experimental import pallas as pl
from jax.experimental.pallas import tpu as pltpu
from jax.sharding import PartitionSpec as P

EPS = 1e-06
OUT_SCALE = 0.8
MESH = pl.DeviceIdType.MESH
HIDDEN = -1e30


def norm_rows(tokens, in_gain):
    floats = tokens.astype(jnp.float32)
    inv_rms = lax.rsqrt(jnp.mean(floats * floats, axis=-1, keepdims=True) + EPS)
    return (floats * inv_rms * in_gain).astype(jnp.bfloat16)


def project(normed, weight):
    order = tuple(range(1, weight.ndim - 1)) + (0, weight.ndim - 1)
    parts = jnp.transpose(weight, order)
    parts = parts.reshape((-1,) + parts.shape[-2:])
    product = jnp.einsum("nd,gdk->gnk", normed, parts, preferred_element_type=jnp.float32)
    return product.astype(jnp.bfloat16)


def meet(axis, count):
    me = lax.axis_index(axis)
    barrier = pltpu.get_barrier_semaphore()
    for step in range(1, count):
        pl.semaphore_signal(
            barrier, inc=1, device_id={axis: lax.rem(me + step, count)}, device_id_type=MESH
        )
    pl.semaphore_wait(barrier, count - 1)
    return me


def mix_maps(first, second, ratio, gain):
    mixed = first - ratio * second
    inv_rms = lax.rsqrt(jnp.mean(mixed * mixed, axis=-1, keepdims=True) + EPS)
    return (mixed * inv_rms * gain * OUT_SCALE).astype(jnp.bfloat16)


SIDE_Y = 4
TILE = 128
EXTRA = 16


def spread(stats, first, groups, width):
    cols = [jnp.broadcast_to(stats[:, i : i + 1], (8, width)) for i in range(first, first + groups)]
    return jnp.concatenate(cols, axis=0)


def pack_columns(columns):
    lane = lax.broadcasted_iota(jnp.int32, (8, TILE), 1)
    out = jnp.zeros((8, TILE), jnp.float32)
    for place, column in columns:
        out = jnp.where(lane == place, column, out)
    return out


def ring_kernel(
    kv_count, fold, ratio, prompt_len, step_lens, gain, queries, new_keys, new_values,
    prompt_keys, prompt_values, cache_keys, cache_values, out,
    q_own, q_all, pairs, kt, values, bias, halves, step_k, step_v, scores, weights,
    sent_v, sent_s, got_v, got_s, far_v, far_s, far_d,
    load_sem, qz_send, qz_recv, qy_send, qy_recv, r_send, r_recv, f_send, f_recv,
):
    ny = SIDE_Y
    nz = kv_count // ny
    tall, dims = queries.shape[1:]
    rows = tall - EXTRA
    wide = values.shape[1]
    cached = bias.shape[1]
    total_keys = values.shape[0]
    slots = step_v.shape[0] // kv_count
    half = 2 * rows
    blocks = rows // 8
    deep = 2 * half
    me = lax.axis_index("kv")
    z = me // ny
    y = lax.rem(me, ny)
    other_z = [lax.rem(z + 1, nz) * ny + y, lax.rem(z + nz - 1, nz) * ny + y]

    loads = [
        pltpu.make_async_copy(prompt_keys, pairs, load_sem.at[0]),
        pltpu.make_async_copy(prompt_values, values.at[pl.ds(0, cached)], load_sem.at[1]),
        pltpu.make_async_copy(cache_keys, step_k, load_sem.at[2]),
        pltpu.make_async_copy(cache_values, step_v, load_sem.at[3]),
    ]
    for copy in loads:
        copy.start()

    barrier = pltpu.get_barrier_semaphore()
    for turn in range(1, nz):
        there = lax.rem(z + turn, nz) * ny + y
        pl.semaphore_signal(barrier, inc=1, device_id={"kv": there}, device_id_type=MESH)
    for turn in range(1, ny):
        there = z * ny + lax.rem(y + turn, ny)
        pl.semaphore_signal(barrier, inc=1, device_id={"kv": there}, device_id_type=MESH)

    extra_row = lax.broadcasted_iota(jnp.int32, (EXTRA, dims), 0)
    for m in range(2):
        q_own[m, :rows] = queries[m, :rows]
        line = queries[m, rows:].astype(jnp.float32)[:1]
        q_own[m, rows:] = jnp.where(extra_row == y, line, 0.0).astype(jnp.bfloat16)
        q_all[m, nz - 1, y] = q_own[m]
        got_v[m, 0] = jnp.zeros(got_v.shape[2:], jnp.bfloat16)
        lane = lax.broadcasted_iota(jnp.int32, (8, TILE), 1)
        spot = jnp.where(lane < 4 * blocks, lax.rem(lane, 2 * blocks), lane - 4 * blocks + blocks - 2)
        for h in range(2):
            got_s[m, 0, h] = jnp.where(spot < blocks, HIDDEN, 0.0)

    pl.semaphore_wait(barrier, nz + ny - 2)

    def to(src, dst, send, recv, device):
        return pltpu.make_async_remote_copy(
            src_ref=src, dst_ref=dst, send_sem=send, recv_sem=recv,
            device_id={"kv": device}, device_id_type=MESH,
        )

    def along_z(m, slot):
        there = lax.rem(z + (1 + slot if m == 0 else nz - 1 - slot), nz) * ny + y
        return to(q_own.at[m], q_all.at[m, slot, y], qz_send.at[m, slot], qz_recv.at[m, slot], there)

    def along_y(m, slot, turn, source):
        return to(
            source, q_all.at[m, slot, y], qy_send.at[m, slot, turn], qy_recv.at[m, slot, y],
            z * ny + lax.rem(y + turn, ny),
        )

    def from_y(m, slot, turn):
        there = lax.rem(y + turn, ny)
        return to(
            q_all.at[m, slot, there], q_all.at[m, slot, there],
            qy_send.at[m, slot, turn], qy_recv.at[m, slot, there], z * ny + there,
        )

    def ring(m, slot, h):
        at = pl.ds(h * half, half + h * EXTRA)
        return (
            to(sent_s.at[m, slot, h], got_s.at[m, slot + 1, h],
               r_send.at[m, slot, h, 0], r_recv.at[m, slot, h, 0], other_z[m]),
            to(sent_v.at[m, slot, at], got_v.at[m, slot + 1, at],
               r_send.at[m, slot, h, 1], r_recv.at[m, slot, h, 1], other_z[m]),
        )

    def final(m, there, i):
        at = pl.ds(pl.multiple_of(there * rows, 32), rows)
        low = pl.ds(deep, EXTRA)
        peer = z * ny + there
        src = (sent_v.at[m, nz - 1, at], sent_s.at[m, nz - 1], sent_v.at[m, nz - 1, low])[i]
        dst = (far_v, far_s, far_d)[i].at[m, y]
        return to(src, dst, f_send.at[m, there, i], f_recv.at[m, y, i], peer)

    def final_from(m, there):
        peer = z * ny + there
        return tuple(
            to(ref.at[m, there], ref.at[m, there], f_send.at[m, there, i], f_recv.at[m, there, i], peer)
            for i, ref in enumerate((far_v, far_s, far_d))
        )

    for m in range(2):
        along_z(m, 0).start()
    for m in range(2):
        along_z(m, 1).start()
    for slot in range(2, nz - 1):
        for m in range(2):
            along_z(m, slot).start()
    for m in range(2):
        for turn in range(1, ny):
            along_y(m, nz - 1, turn, q_own.at[m]).start()

    def fan_out(slot):
        for m in range(2):
            along_z(m, slot).wait_recv()
            for turn in range(1, ny):
                along_y(m, slot, turn, q_all.at[m, slot, y]).start()

    fan_out(0)

    key_lane = lax.broadcasted_iota(jnp.int32, (1, cached), 1)
    bias[...] = jnp.where(me * cached + key_lane < prompt_len[0], 0.0, HIDDEN)
    values[cached : cached + rows] = new_values[:rows]
    values[cached + rows :] = jnp.zeros((total_keys - cached - rows, wide), jnp.bfloat16)
    for m in range(2):
        fresh = jnp.concatenate(
            [new_keys[m, :rows].astype(jnp.float32), jnp.zeros((TILE - rows, dims), jnp.float32)], axis=0
        )
        kt[m, :, cached:] = jnp.transpose(fresh).astype(jnp.bfloat16)
    up = lax.broadcasted_iota(jnp.int32, (2 * TILE, 2 * TILE), 0)
    across = lax.broadcasted_iota(jnp.int32, (2 * TILE, 2 * TILE), 1)
    sort = jnp.where(across < TILE, 2 * across, 2 * across - 2 * TILE + 1) == up
    sort = sort.astype(jnp.float32).astype(jnp.bfloat16)
    up = lax.broadcasted_iota(jnp.int32, (2 * TILE, TILE), 0)
    across = lax.broadcasted_iota(jnp.int32, (2 * TILE, TILE), 1)
    halves[...] = (up // 2 == across).astype(jnp.float32).astype(jnp.bfloat16)
    loads[0].wait()

    def split(i, carry):
        block = pairs[pl.ds(pl.multiple_of(i * 2 * TILE, 2 * TILE), 2 * TILE), :]
        turned = lax.dot_general(
            block, sort, (((0,), (0,)), ((), ())), preferred_element_type=jnp.float32
        ).astype(jnp.bfloat16)
        at = pl.ds(pl.multiple_of(i * TILE, TILE), TILE)
        kt[0, :, at] = turned[:, :TILE]
        kt[1, :, at] = turned[:, TILE:]
        return carry

    lax.fori_loop(0, cached // TILE, split, 0)
    for copy in loads[1:]:
        copy.wait()

    def score(m, h, slot, off):
        q = q_all[m, slot, 2 * h : 2 * h + 2, :rows].reshape(half, dims)
        buf = (2 * m + h) % 2
        best = None
        for c in range(0, cached, 256):
            s = jnp.dot(q, kt[m, :, c : c + 256], preferred_element_type=jnp.float32)
            s = s + bias[:, c : c + 256]
            scores[buf, :, c : c + 256] = s
            for j in range(0, 256, TILE):
                p = s[:, j : j + TILE]
                best = p if best is None else jnp.maximum(best, p)
        tail = jnp.dot(q, kt[m, :, cached:], preferred_element_type=jnp.float32)
        lane = lax.broadcasted_iota(jnp.int32, tail.shape, 1)
        row = lax.broadcasted_iota(jnp.int32, tail.shape, 0)
        gap = jnp.where(lane < rows, lane - row, 1 << 20)
        tail = jnp.where(gap <= off, tail, HIDDEN)
        scores[buf, :, cached:] = tail
        best = jnp.maximum(best, tail)
        return jnp.max(best, axis=1, keepdims=True)

    def weigh(m, h, top):
        buf = (2 * m + h) % 2
        part = None
        for c in range(0, total_keys, TILE):
            w = jnp.exp2((scores[buf, :, c : c + TILE] - top) * fold)
            weights[buf, :, c : c + TILE] = w.astype(jnp.bfloat16)
            part = w if part is None else part + w
        total = jnp.sum(part, axis=1, keepdims=True)
        return jnp.dot(weights[buf], values[...], preferred_element_type=jnp.float32), total

    def decode(m, slot, home):
        q = q_all[m, slot, 0, rows:].astype(jnp.float32)
        for there in range(1, ny):
            q = q + q_all[m, slot, there, rows:].astype(jnp.float32)
        qb = q.astype(jnp.bfloat16)
        row = lax.broadcasted_iota(jnp.int32, (EXTRA, 2 * slots), 0)
        lane = lax.broadcasted_iota(jnp.int32, (EXTRA, 2 * slots), 1)
        s = jnp.zeros((EXTRA, 2 * slots), jnp.float32)
        lens = jnp.zeros((EXTRA, 2 * slots), jnp.int32)
        for there in range(ny):
            seq = home * ny + there
            at = pl.ds(pl.multiple_of(seq * 2 * slots, 2 * slots), 2 * slots)
            one = lax.dot_general(
                qb, step_k[at, :], (((1,), (1,)), ((), ())), preferred_element_type=jnp.float32
            )
            s = jnp.where(row == there, one, s)
            lens = jnp.where(row == there, step_lens[seq], lens)
        seen = (lax.rem(lane, 2) == m) & (me * slots + lane // 2 < lens)
        s = jnp.where(seen, s, HIDDEN)
        own = jnp.sum(q * new_keys[m, rows:].astype(jnp.float32)[:1], axis=1, keepdims=True)
        mine = jnp.where(slot == nz - 1, y, EXTRA)
        own = jnp.where(row[:, :1] == mine, own, HIDDEN)
        top = jnp.maximum(jnp.max(s, axis=1, keepdims=True), own)
        w = jnp.exp2((s - top) * fold)
        own_w = jnp.exp2((own - top) * fold)
        total = jnp.sum(w, axis=1, keepdims=True) + own_w
        packed = jnp.dot(
            w.astype(jnp.bfloat16), halves[...], preferred_element_type=jnp.float32
        ).astype(jnp.bfloat16)
        wide_row = lax.broadcasted_iota(jnp.int32, (EXTRA, wide), 0)
        summed = jnp.zeros((EXTRA, wide), jnp.float32)
        for there in range(ny):
            seq = home * ny + there
            at = pl.ds(pl.multiple_of(seq * slots, slots), slots)
            one = jnp.dot(packed, step_v[at, :], preferred_element_type=jnp.float32)
            summed = jnp.where(wide_row == there, one, summed)
        own_w = own_w.astype(jnp.bfloat16).astype(jnp.float32)
        summed = summed + own_w * new_values[rows:].astype(jnp.float32)[:1]
        return top, total, summed

    def join(m, h, slot, top, total, summed):
        at = pl.ds(h * half, half + h * EXTRA)
        old = got_s[m, slot, h]
        places = [(2 * blocks * j, blocks) for j in range(2)] + [(4 * blocks, 2)] * h
        old_top = jnp.concatenate([spread(old, first, n, TILE) for first, n in places], axis=0)
        old_total = jnp.concatenate([spread(old, first + n, n, TILE) for first, n in places], axis=0)
        best = jnp.maximum(old_top, top)
        old_scale = jnp.exp2((old_top - best) * fold)
        new_scale = jnp.exp2((top - best) * fold)
        norm = old_total * old_scale + total * new_scale
        for c in range(0, wide, TILE):
            mixed = got_v[m, slot, at, c : c + TILE].astype(jnp.float32) * old_scale
            mixed = mixed + summed[:, c : c + TILE] * new_scale
            sent_v[m, slot, at, c : c + TILE] = mixed.astype(jnp.bfloat16)
        columns = []
        line = 0
        for first, n in places:
            for i in range(n):
                columns.append((first + i, best[line : line + 8]))
                columns.append((first + n + i, norm[line : line + 8]))
                line += 8
        sent_s[m, slot, h] = pack_columns(columns)

    units = [(m, h) for m in range(2) for h in range(2)]

    def turn_step(slot, carry):
        @pl.when(slot < nz - 2)
        def _():
            fan_out(slot + 1)

        for m in range(2):
            for turn in range(1, ny):
                from_y(m, slot, turn).wait_recv()
        homes = [lax.rem(z + nz - 1 - slot, nz), lax.rem(z + 1 + slot, nz)]
        offs = [[(homes[m] * ny + 2 * h - me) * rows for h in range(2)] for m in range(2)]
        tops = [None] * len(units)
        tops[0] = score(0, 0, slot, offs[0][0])
        for u, (m, h) in enumerate(units):
            if u + 1 < len(units):
                m2, h2 = units[u + 1]
                tops[u + 1] = score(m2, h2, slot, offs[m2][h2])
            top = tops[u]
            summed, total = weigh(m, h, top)
            if h == 1:
                low = decode(m, slot, homes[m])
                top, total, summed = [
                    jnp.concatenate([p, q], axis=0) for p, q in zip((top, total, summed), low)
                ]

            @pl.when(slot > 0)
            def _():
                for copy in ring(m, slot - 1, h):
                    copy.wait_recv()

            join(m, h, slot, top, total, summed)

            @pl.when(slot < nz - 1)
            def _():
                for copy in ring(m, slot, h):
                    copy.start()

            @pl.when(slot == nz - 1)
            def _():
                for there in range(ny):
                    @pl.when(y != there)
                    def _():
                        picks = [0] * (there // 2 == h) + [1, 2] * h
                        for i in picks:
                            final(m, there, i).start()
        return carry

    lax.fori_loop(0, nz, turn_step, 0)

    for m in range(2):
        for turn in range(1, ny):
            for copy in final_from(m, lax.rem(y + turn, ny)):
                copy.wait_recv()
    odd = lax.rem(y, 2) == 1

    def own_half(stats):
        return jnp.where(odd, pltpu.roll(stats, TILE - 2 * blocks, 1), stats)

    def merge(vals, tops, totals):
        best = functools.reduce(jnp.maximum, tops)
        scales = [jnp.exp2((t - best) * fold) for t in tops]
        norm = functools.reduce(jnp.add, [a * b for a, b in zip(scales, totals)])
        total = functools.reduce(jnp.add, [a * b.astype(jnp.float32) for a, b in zip(scales, vals)])
        return total / norm

    peers = [lax.rem(y + turn, ny) for turn in range(1, ny)]
    maps_out = []
    for m in range(2):
        vals = [sent_v[m, nz - 1, deep:]] + [far_d[m, there] for there in peers]
        stats = [sent_s[m, nz - 1, 1]] + [far_s[m, there, 1] for there in peers]
        maps_out.append(
            merge(
                vals,
                [spread(s, 4 * blocks, 2, wide) for s in stats],
                [spread(s, 4 * blocks + 2, 2, wide) for s in stats],
            )
        )
    lines = mix_maps(maps_out[0], maps_out[1], ratio[0, 0], gain[...]).astype(jnp.float32)
    place = lax.broadcasted_iota(jnp.int32, lines.shape, 0)
    line = jnp.sum(jnp.where(place == y, lines, 0.0), axis=0, keepdims=True)
    out[rows:, :] = jnp.where(place == 0, line, 0.0).astype(jnp.bfloat16)

    stats = [
        [own_half(sent_s[m, nz - 1, y // 2])] + [own_half(far_s[m, there, y // 2]) for there in peers]
        for m in range(2)
    ]
    cut = 32
    for j in range(rows // cut):
        maps_out = []
        for m in range(2):
            at = pl.ds(pl.multiple_of(y * rows + j * cut, cut), cut)
            vals = [sent_v[m, nz - 1, at, :]]
            vals += [far_v[m, there, j * cut : (j + 1) * cut, :] for there in peers]
            first = j * cut // 8
            maps_out.append(
                merge(
                    vals,
                    [spread(s, first, cut // 8, wide) for s in stats[m]],
                    [spread(s, blocks + first, cut // 8, wide) for s in stats[m]],
                )
            )
        out[j * cut : (j + 1) * cut, :] = mix_maps(maps_out[0], maps_out[1], ratio[0, 0], gain[...])

    for m in range(2):
        for there in range(ny):
            @pl.when(y != there)
            def _():
                for i in range(3):
                    final(m, there, i).wait_send()
        for turn in range(1, ny):
            along_y(m, nz - 1, turn, q_own.at[m]).wait_send()

    def drain(slot, carry):
        for m in range(2):
            along_z(m, slot).wait_send()
            for turn in range(1, ny):
                along_y(m, slot, turn, q_own.at[m]).wait_send()
            for h in range(2):
                for copy in ring(m, slot, h):
                    copy.wait_send()
        return carry

    lax.fori_loop(0, nz - 1, drain, 0)


def ring_attend(
    ratio, prompt_len, step_lens, gain, queries, new_keys, new_values,
    prompt_keys, prompt_values, cache_keys, cache_values, kv_count, collective,
):
    tall, dims = queries.shape[1:]
    rows = tall - EXTRA
    wide = new_values.shape[1]
    cached = prompt_values.shape[0]
    keys = cached + TILE
    ny = SIDE_Y
    nz = kv_count // ny
    deep = ny * rows + EXTRA
    smem = pl.BlockSpec(memory_space=pltpu.SMEM)
    vmem = pl.BlockSpec(memory_space=pltpu.VMEM)
    far = pl.BlockSpec(memory_space=pl.ANY)
    dma = pltpu.SemaphoreType.DMA
    half = jnp.bfloat16
    fold = dims ** (-0.5) * math.log2(math.e)
    return pl.pallas_call(
        functools.partial(ring_kernel, kv_count, fold),
        out_shape=jax.ShapeDtypeStruct((tall, wide), half),
        in_specs=[smem] * 3 + [vmem] * 4 + [far] * 4,
        out_specs=vmem,
        scratch_shapes=[
            pltpu.VMEM((2, tall, dims), half),
            pltpu.VMEM((2, nz, ny, tall, dims), half),
            pltpu.VMEM(prompt_keys.shape, half),
            pltpu.VMEM((2, dims, keys), half),
            pltpu.VMEM((keys, wide), half),
            pltpu.VMEM((1, cached), jnp.float32),
            pltpu.VMEM((2 * TILE, TILE), half),
            pltpu.VMEM(cache_keys.shape, half),
            pltpu.VMEM(cache_values.shape, half),
            pltpu.VMEM((2, 2 * rows, keys), jnp.float32),
            pltpu.VMEM((2, 2 * rows, keys), half),
            pltpu.VMEM((2, nz, deep, wide), half),
            pltpu.VMEM((2, nz, 2, 8, TILE), jnp.float32),
            pltpu.VMEM((2, nz, deep, wide), half),
            pltpu.VMEM((2, nz, 2, 8, TILE), jnp.float32),
            pltpu.VMEM((2, ny, rows, wide), half),
            pltpu.VMEM((2, ny, 2, 8, TILE), jnp.float32),
            pltpu.VMEM((2, ny, EXTRA, wide), half),
            dma((4,)),
            dma((2, nz)), dma((2, nz)),
            dma((2, nz, ny)), dma((2, nz, ny)),
            dma((2, nz, 2, 2)), dma((2, nz, 2, 2)),
            dma((2, ny, 3)), dma((2, ny, 3)),
        ],
        compiler_params=pltpu.CompilerParams(
            collective_id=collective, has_side_effects=True, vmem_limit_bytes=56 * 1024 * 1024
        ),
        name="ring_attend",
    )(
        ratio, prompt_len, step_lens, gain, queries, new_keys, new_values,
        prompt_keys, prompt_values, cache_keys, cache_values,
    )


def project_out_kernel(axis, count, heads, weight, out, terms, pair, half, far, d_send, d_recv, x_send, x_recv):
    me = lax.axis_index(axis)
    chips = count // 2
    chip, core = me // 2, lax.rem(me, 2)
    meet(axis, count)
    wide = out.shape[1]
    for target in range(count):
        terms[target] = jnp.dot(
            heads[...], weight[:, target * wide : target * wide + wide], preferred_element_type=jnp.float32
        ).astype(jnp.bfloat16)
    near = []
    for turn in range(1, chips + 1):
        there = lax.rem(chip + turn, chips)
        copy = pltpu.make_async_remote_copy(
            src_ref=terms.at[there * 2 + 1 - core],
            dst_ref=pair.at[there],
            send_sem=d_send.at[turn],
            recv_sem=d_recv.at[turn],
            device_id={axis: chip * 2 + 1 - core},
            device_id_type=MESH,
        )
        copy.start()
        near.append(copy)
    away = []
    for turn in range(1, chips + 1):
        near[turn - 1].wait()
        there = lax.rem(chip + turn, chips)
        both = terms[there * 2 + core].astype(jnp.float32) + pair[there].astype(jnp.float32)
        if turn == chips:
            total = both
            for copy in away:
                copy.wait()
            for slot in range(1, chips):
                total = total + far[slot].astype(jnp.float32)
            out[...] = total.astype(jnp.bfloat16)
        else:
            half[turn] = both.astype(jnp.bfloat16)
            copy = pltpu.make_async_remote_copy(
                src_ref=half.at[turn],
                dst_ref=far.at[turn],
                send_sem=x_send.at[turn],
                recv_sem=x_recv.at[turn],
                device_id={axis: there * 2 + core},
                device_id_type=MESH,
            )
            copy.start()
            away.append(copy)


def project_out(heads, weight, axis, count, collective):
    wide = weight.shape[1] // count
    rows = heads.shape[0]
    chips = count // 2
    vmem = pl.BlockSpec(memory_space=pltpu.VMEM)
    return pl.pallas_call(
        functools.partial(project_out_kernel, axis, count),
        out_shape=jax.ShapeDtypeStruct((rows, wide), jnp.bfloat16),
        in_specs=[vmem, vmem],
        out_specs=vmem,
        scratch_shapes=[
            pltpu.VMEM((count, rows, wide), jnp.bfloat16),
            pltpu.VMEM((chips, rows, wide), jnp.bfloat16),
            pltpu.VMEM((chips, rows, wide), jnp.bfloat16),
            pltpu.VMEM((chips, rows, wide), jnp.bfloat16),
            pltpu.SemaphoreType.DMA((chips + 1,)),
            pltpu.SemaphoreType.DMA((chips + 1,)),
            pltpu.SemaphoreType.DMA((chips + 1,)),
            pltpu.SemaphoreType.DMA((chips + 1,)),
        ],
        compiler_params=pltpu.CompilerParams(
            collective_id=collective, has_side_effects=True, vmem_limit_bytes=56 * 1024 * 1024
        ),
        name="project_out",
    )(heads, weight)


def on_device(
    kv_count,
    tp_count,
    piece_tokens,
    step_tokens,
    in_gain,
    w_query,
    w_key,
    w_value,
    w_out,
    mix_ratio,
    out_gain,
    prompt_keys,
    prompt_values,
    step_cache_keys,
    step_cache_values,
    prompt_len,
    step_lens,
):
    piece_dev = piece_tokens.shape[0]
    step_dev = step_tokens.shape[0]
    heads, maps, dims = w_query.shape[1:]
    wide = w_value.shape[-1]
    padded = -(-(piece_dev + step_dev) // EXTRA) * EXTRA
    spare = jnp.zeros((padded - piece_dev - step_dev, piece_tokens.shape[1]), jnp.bfloat16)
    all_rows = jnp.concatenate([piece_tokens, step_tokens, spare], axis=0)
    normed = norm_rows(all_rows, in_gain)
    queries = project(normed, w_query)
    key_rows = project(normed, w_key)
    value_rows = project(normed, w_value)
    end = piece_dev + step_dev

    def rows_of(flat, start, stop, extra):
        return jnp.transpose(flat[:, start:stop], (1, 0, 2)).reshape((stop - start,) + extra)

    piece_k = rows_of(key_rows, 0, piece_dev, (heads, maps, dims))
    step_k = rows_of(key_rows, piece_dev, end, (heads, maps, dims))
    piece_v = rows_of(value_rows, 0, piece_dev, (heads, wide))
    step_v = rows_of(value_rows, piece_dev, end, (heads, wide))
    flat_heads = ring_attend(
        mix_ratio[None, :],
        prompt_len,
        step_lens,
        out_gain[None, :],
        queries,
        key_rows,
        value_rows[0],
        prompt_keys.reshape(-1, dims),
        prompt_values.reshape(-1, wide),
        step_cache_keys.reshape(-1, dims),
        step_cache_values.reshape(-1, wide),
        kv_count,
        1,
    )
    mixed = project_out(flat_heads, w_out.reshape(-1, w_out.shape[-1]), "tp", tp_count, 2)
    return (mixed[:piece_dev], mixed[piece_dev:end], piece_k, piece_v, step_k, step_v)


def solution(mesh):
    in_specs = (
        P("kv", None),
        P("kv", None),
        P(),
        P(None, "tp", None, None),
        P(None, "tp", None, None),
        P(None, "tp", None),
        P("tp", None, None),
        P("tp"),
        P(),
        P("kv", "tp", None, None),
        P("kv", "tp", None),
        P(None, "kv", "tp", None, None),
        P(None, "kv", "tp", None),
        P(),
        P(),
    )
    out_specs = (
        P("kv", "tp"),
        P("kv", "tp"),
        P("kv", "tp", None, None),
        P("kv", "tp", None),
        P("kv", "tp", None, None),
        P("kv", "tp", None),
    )
    return jax.shard_map(
        functools.partial(on_device, mesh.shape["kv"], mesh.shape["tp"]),
        mesh=mesh, in_specs=in_specs, out_specs=out_specs, check_vma=False
    )
```

time: 129 us -> 102 us (0.79)
  Pallas kernels: 98.4 us -> 87.5 us
  other arithmetic: 7.06 us -> 1.68 us
  local copies, waits for them, and re-layouts: 11 us -> 5.8 us
  matrix products: 10.1 us -> 4.98 us
    pallas_call x1 -> x0, Pallas kernels: 15.9 us -> none  [gather_rows(): pl.pallas_call(functools.partial(gather_kernel, axis, count), out_shape=j...]
    pallas_call x1, Pallas kernels: 62.2 us -> 67.3 us  [ring_attend(): pl.pallas_call(functools.partial(ring_kernel, kv_count, fold), out_shape=...]
    dot_general x2 -> x0, matrix products: 4.8 us -> none  [the longest x1 2.76 us: on_device(): jnp.einsum('bhcd,bkhcd->bhck', step_q, step_cache_keys, preferred_element...]
    concatenate x1 -> x0, other arithmetic: 2.35 us -> none  [on_device(): jnp.concatenate([prompt_values[:, 0], value_rows[0, :piece_dev], jnp.zero...]
    concatenate x2 -> x0, local copies, waits for them, and re-layouts: 1.91 us -> none  [the longest x1 1.84 us: on_device(): jnp.concatenate([keys, fresh_k, jnp.zeros((parts, dims, spare_keys), jnp....]
    unnamed x14 -> x18, local copies, waits for them, and re-layouts: 3.34 us -> 1.71 us
where the time goes in v2:
time: 102 us
  Pallas kernels  87.5 us (86%)
  local copies, waits for them, and re-layouts  5.8 us (6%)
  matrix products  4.98 us (5%)
  between operations  2.02 us (2%)
  other arithmetic  1.68 us (2%)
    pallas_call x1, Pallas kernels, ring_attend(): pl.pallas_call(functools.partial(ring_kernel, kv_count, fold), out_shape=...  67.3 us
    pallas_call x1, Pallas kernels, project_out(): pl.pallas_call(functools.partial(project_out_kernel, axis, count), out_sh...  20.3 us
    dot_general x3, matrix products, project(): jnp.einsum('nd,gdk->gnk', normed, parts, preferred_element_type=jnp.float32)  4.98 us

profile of v2, /device:TPU:1, one launch (start us, length us, event | category | flops | bytes accessed | tf_op | source)
XLA Modules:
  0.0 102.0 jit_solution(18398276089080214615)
XLA Ops:
  0.6 0.0 copy-start
  0.7 0.1 pad.2.clone
  0.7 1.7 %fusion.6 = f32[112]{0:T(128)S(1)} fusion(bf16[1,4096]{1,0:T(2,128)(2,1)} %param.16, bf16[96,4096]{1,0:T(8,128)(2,1)} %param.15, bf16[112]{0:T(256)(128)(2,1)S(1)} %pad.2.clone), kind=kLoop, calls=%fused_computation.8 | loop fusion | flops 3669904 | bytes 795296 | tf_op jit(solution)/shard_map/reduce_sum | solution.py:19
  2.4 0.1 copy-done
  2.5 0.0 copy-start.1
  2.5 0.0 copy-start.4
  2.5 0.0 copy-start.5
  2.5 0.0 copy-start.7
  2.5 2.6 %fusion.18.new_keys = bf16[2,112,128]{2,1,0:T(8,128)(2,1)} fusion(bf16[2,4096,128]{2,0,1:T(2,128)(2,1)S(1)} %bitcast.42, f32[4096]{0:T(1024)} %param.17, f32[112]{0:T(128)S(1)} %add_rsqrt_fusion, bf16[1,4096]{1,0:T(2,128)(2,1)} %param.16, bf16[96,4096]{1,0:T(8,128)(2,1)} %param.15, bf16[112]{0:T(256)(128)(2,1)S(1)} %pad.2.clone), kind=kOutput, calls=%fused_computation.14 | convolution fusion | flops 239038464 | bytes 2966176 | tf_op jit(solution)/shard_map/nd,gdk->gnk/dot_general | solution.py:27
  5.1 0.0 copy-done.1
  5.1 0.0 copy-done.4
  5.1 0.0 copy-done.5
  5.1 0.0 copy-done.7
  5.1 0.0 copy-start.6
  5.1 1.2 %fusion.15.new_values = bf16[112,256]{1,0:T(8,128)(2,1)} fusion(bf16[4096,1,256]{2,0,1:T(8,128)(2,1)S(1)} %copy-done.5, f32[4096]{0:T(1024)S(1)} %copy-done.7, f32[112]{0:T(128)S(1)} %add_rsqrt_fusion, bf16[1,4096]{1,0:T(2,128)(2,1)S(1)} %copy-done.4, bf16[96,4096]{1,0:T(8,128)(2,1)S(1)} %copy-done.1, bf16[112]{0:T(256)(128)(2,1)S(1)} %pad.2.clone), kind=kOutput, calls=%fused_computation.13 | convolution fusion | flops 239038464 | bytes 2966176 | tf_op jit(solution)/shard_map/nd,gdk->gnk/dot_general | solution.py:27
  6.2 0.4 copy-done.6
  6.7 1.3 %fusion.21.queries = bf16[2,112,128]{2,1,0:T(8,128)(2,1)} fusion(bf16[2,4096,128]{2,0,1:T(2,128)(2,1)S(1)} %bitcast.51, f32[4096]{0:T(1024)S(1)} %copy-done.7, f32[112]{0:T(128)S(1)} %add_rsqrt_fusion, bf16[1,4096]{1,0:T(2,128)(2,1)S(1)} %copy-done.4, bf16[96,4096]{1,0:T(8,128)(2,1)S(1)} %copy-done.1, bf16[112]{0:T(256)(128)(2,1)S(1)} %pad.2.clone), kind=kOutput, calls=%fused_computation.15 | convolution fusion | flops 239038464 | bytes 2966176 | tf_op jit(solution)/shard_map/nd,gdk->gnk/dot_general | solution.py:27
  9.2 67.3 %ring_attend.1.heads = bf16[112,256]{1,0:T(8,128)(2,1)} custom-call(f32[1,1]{1,0:T(1,128)} %bitcast.41.ratio, s32[1]{0:T(128)S(6)} %copy.43.prompt_len, s32[32]{0:T(128)} %step_lens.1, f32[1,256]{1,0:T(1,128)} %bitcast.50, bf16[2,112,128]{2,1,0:T(8,128)(2,1)} %fusion.21.queries, bf16[2,112,128]{2,1,0:T(8,128)(2,1)} %fusion.18.new_keys, ...), custom_call_target="tpu_custom_call" | custom-call | tf_op jit(solution)/shard_map/ring_attend/pallas_call | solution.py:455
  76.5 0.0 copy-start.3
  76.5 0.0 copy-start.2
  76.6 20.3 %project_out.1 = bf16[112,512]{1,0:T(8,128)(2,1)} custom-call(bf16[112,256]{1,0:T(8,128)(2,1)} %ring_attend.1.heads, bf16[256,4096]{1,0:T(8,128)(2,1)} %bitcast.45), custom_call_target="tpu_custom_call" | custom-call | tf_op jit(solution)/shard_map/project_out/pallas_call | solution.py:549
  96.8 1.5 %slice.18 = bf16[96,512]{1,0:T(8,128)(2,1)} slice(bf16[112,512]{1,0:T(8,128)(2,1)} %project_out.1), slice={[0:96], [0:512]} | slice | bytes 196608 | tf_op jit(solution)/shard_map/slice | solution.py:626
  98.4 1.3 %slice.19 = bf16[1,512]{1,0:T(2,128)(2,1)} slice(bf16[112,512]{1,0:T(8,128)(2,1)} %project_out.1), slice={[96:97], [0:512]} | slice | bytes 2048 | tf_op jit(solution)/shard_map/slice | solution.py:626
  99.6 0.0 copy-done.3
  99.6 0.7 copy.26
  100.3 0.0 copy-done.2
  100.3 0.6 slice_bitcast_fusion
  100.9 0.5 copy.41
  101.4 0.6 slice.27
  (4 shorter events, 0.0 us)
Async XLA Ops:
  0.6 1.8 %copy-start = (bf16[4096,1,2,128]{3,2,1,0:T(2,128)(2,1)S(1)}, bf16[4096,1,2,128]{3,2,1,0:T(2,128)(2,1)}, u32[]{:S(2)}) copy-start(bf16[4096,1,2,128]{3,2,1,0:T(2,128)(2,1)} %param.19) | copy-start | bytes 6291460
  2.5 2.6 %copy-start.1 = (bf16[96,4096]{1,0:T(8,128)(2,1)S(1)}, bf16[96,4096]{1,0:T(8,128)(2,1)}, u32[]{:S(2)}) copy-start(bf16[96,4096]{1,0:T(8,128)(2,1)} %param.15) | copy-start | bytes 2359300
  2.5 2.6 %copy-start.4 = (bf16[1,4096]{1,0:T(2,128)(2,1)S(1)}, bf16[1,4096]{1,0:T(2,128)(2,1)}, u32[]{:S(2)}) copy-start(bf16[1,4096]{1,0:T(2,128)(2,1)} %param.16) | copy-start | bytes 24580
  2.5 2.6 %copy-start.5 = (bf16[4096,1,256]{2,0,1:T(8,128)(2,1)S(1)}, bf16[4096,1,256]{2,0,1:T(8,128)(2,1)}, u32[]{:S(2)}) copy-start(bf16[4096,1,256]{2,0,1:T(8,128)(2,1)} %param.20) | copy-start | bytes 6291460
  2.5 2.6 %copy-start.7 = (f32[4096]{0:T(1024)S(1)}, f32[4096]{0:T(1024)}, u32[]{:S(2)}) copy-start(f32[4096]{0:T(1024)} %param.17) | copy-start | bytes 49156
  5.1 1.6 %copy-start.6 = (bf16[4096,1,2,128]{3,2,1,0:T(2,128)(2,1)S(1)}, bf16[4096,1,2,128]{3,2,1,0:T(2,128)(2,1)}, u32[]{:S(2)}) copy-start(bf16[4096,1,2,128]{3,2,1,0:T(2,128)(2,1)} %param.18) | copy-start | bytes 6291460
  76.5 23.1 %copy-start.3 = (bf16[2,112,128]{2,1,0:T(8,128)(2,1)S(1)}, bf16[2,112,128]{2,1,0:T(8,128)(2,1)}, u32[]{:S(2)}) copy-start(bf16[2,112,128]{2,1,0:T(8,128)(2,1)} %fusion.18.new_keys) | copy-start | bytes 172036
  76.5 23.8 %copy-start.2 = (bf16[112,256]{1,0:T(8,128)(2,1)S(1)}, bf16[112,256]{1,0:T(8,128)(2,1)}, u32[]{:S(2)}) copy-start(bf16[112,256]{1,0:T(8,128)(2,1)} %fusion.15.new_values) | copy-start | bytes 172036

commit v3 on v2

--- a/solution.py
+++ b/solution.py
@@ -14,29 +14,38 @@
 HIDDEN = -1e30
 
 
-def norm_rows(tokens, in_gain):
-    floats = tokens.astype(jnp.float32)
-    inv_rms = lax.rsqrt(jnp.mean(floats * floats, axis=-1, keepdims=True) + EPS)
-    return (floats * inv_rms * in_gain).astype(jnp.bfloat16)
-
-
-def project(normed, weight):
-    order = tuple(range(1, weight.ndim - 1)) + (0, weight.ndim - 1)
-    parts = jnp.transpose(weight, order)
-    parts = parts.reshape((-1,) + parts.shape[-2:])
-    product = jnp.einsum("nd,gdk->gnk", normed, parts, preferred_element_type=jnp.float32)
-    return product.astype(jnp.bfloat16)
-
-
-def meet(axis, count):
-    me = lax.axis_index(axis)
-    barrier = pltpu.get_barrier_semaphore()
-    for step in range(1, count):
-        pl.semaphore_signal(
-            barrier, inc=1, device_id={axis: lax.rem(me + step, count)}, device_id_type=MESH
-        )
-    pl.semaphore_wait(barrier, count - 1)
-    return me
+def finish_kernel(mixed, line, keys, vals, piece_out, step_out, piece_k, piece_v, step_k, step_v):
+    rows = piece_out.shape[0]
+    piece_out[...] = mixed[...]
+    step_out[...] = line[...]
+    piece_v[...] = vals[:rows]
+    step_v[...] = vals[rows:].astype(jnp.float32)[:1].astype(jnp.bfloat16)
+    up = lax.broadcasted_iota(jnp.int32, (2 * rows, rows), 0)
+    right = lax.broadcasted_iota(jnp.int32, (2 * rows, rows), 1)
+    total = None
+    for m in range(2):
+        pick = (up == 2 * right + m).astype(jnp.float32).astype(jnp.bfloat16)
+        part = jnp.dot(pick, keys[m, :rows], preferred_element_type=jnp.float32)
+        total = part if total is None else total + part
+    piece_k[...] = total.astype(jnp.bfloat16)
+    both = [keys[m, rows:].astype(jnp.float32)[:1] for m in range(2)]
+    step_k[...] = jnp.concatenate(both, axis=0).astype(jnp.bfloat16)
+
+
+def finish(mixed, line, keys, vals):
+    rows, span = mixed.shape
+    dims = keys.shape[-1]
+    wide = vals.shape[-1]
+    vmem = pl.BlockSpec(memory_space=pltpu.VMEM)
+    shapes = [(rows, span), (1, span), (2 * rows, dims), (rows, wide), (2, dims), (1, wide)]
+    return pl.pallas_call(
+        finish_kernel,
+        out_shape=[jax.ShapeDtypeStruct(shape, jnp.bfloat16) for shape in shapes],
+        in_specs=[vmem] * 4,
+        out_specs=[vmem] * 6,
+        compiler_params=pltpu.CompilerParams(vmem_limit_bytes=62 * 1024 * 1024),
+        name="finish",
+    )(mixed, line, keys, vals)
 
 
 def mix_maps(first, second, ratio, gain):
@@ -64,15 +73,18 @@
 
 
 def ring_kernel(
-    kv_count, fold, ratio, prompt_len, step_lens, gain, queries, new_keys, new_values,
-    prompt_keys, prompt_values, cache_keys, cache_values, out,
-    q_own, q_all, pairs, kt, values, bias, halves, step_k, step_v, scores, weights,
-    sent_v, sent_s, got_v, got_s, far_v, far_s, far_d,
+    kv_count, tp_count, fold, step_lens, ratio, prompt_len, gain,
+    piece, step, scale_in, w_query, w_key, w_value,
+    prompt_keys, prompt_values, cache_keys, cache_values, w_out, piece_out, step_out, new_keys, new_values,
+    tokens, step_token, scales, wq, wk, wv, normed, spaced, both, q_own, q_all, pairs, kt, values, bias, halves, step_k, step_v, scores, weights,
+    sent_v, sent_s, got_v, got_s, far_v, far_s, far_d, cols, heads,
     load_sem, qz_send, qz_recv, qy_send, qy_recv, r_send, r_recv, f_send, f_recv,
+    c_send, c_recv, h_send, h_recv, d_send, d_recv,
 ):
     ny = SIDE_Y
     nz = kv_count // ny
-    tall, dims = queries.shape[1:]
+    tall, dims = new_keys.shape[1:]
+    model = piece.shape[1]
     rows = tall - EXTRA
     wide = values.shape[1]
     cached = bias.shape[1]
@@ -85,37 +97,78 @@
     z = me // ny
     y = lax.rem(me, ny)
     other_z = [lax.rem(z + 1, nz) * ny + y, lax.rem(z + nz - 1, nz) * ny + y]
-
-    loads = [
-        pltpu.make_async_copy(prompt_keys, pairs, load_sem.at[0]),
-        pltpu.make_async_copy(prompt_values, values.at[pl.ds(0, cached)], load_sem.at[1]),
-        pltpu.make_async_copy(cache_keys, step_k, load_sem.at[2]),
-        pltpu.make_async_copy(cache_values, step_v, load_sem.at[3]),
+    mine = lax.axis_index("tp")
+    chips = tp_count // 2
+    chip = mine // 2
+    core = lax.rem(mine, 2)
+    span = piece_out.shape[1]
+
+    def load(i, source, target):
+        copy = pltpu.make_async_copy(source, target, load_sem.at[i])
+        copy.start()
+        return copy
+
+    first_loads = [
+        load(0, piece, tokens.at[pl.ds(0, rows)]),
+        load(1, step, step_token),
+        load(2, scale_in, scales),
     ]
-    for copy in loads:
-        copy.start()
+    wq_load = load(3, w_query, wq)
+    wk_load = load(4, w_key, wk)
+    pairs_load = load(5, prompt_keys, pairs)
+    wv_load = load(6, w_value, wv)
+    last_loads = [
+        load(7, prompt_values, values.at[pl.ds(0, cached)]),
+        load(8, cache_keys, step_k),
+        load(9, cache_values, step_v),
+        load(10, w_out.at[:, pl.ds(pl.multiple_of(mine * span, span), span)], cols.at[mine]),
+    ]
 
     barrier = pltpu.get_barrier_semaphore()
-    for turn in range(1, nz):
-        there = lax.rem(z + turn, nz) * ny + y
+    for there in other_z + [z * ny + lax.rem(y + turn, ny) for turn in range(1, ny)]:
         pl.semaphore_signal(barrier, inc=1, device_id={"kv": there}, device_id_type=MESH)
-    for turn in range(1, ny):
-        there = z * ny + lax.rem(y + turn, ny)
-        pl.semaphore_signal(barrier, inc=1, device_id={"kv": there}, device_id_type=MESH)
-
-    extra_row = lax.broadcasted_iota(jnp.int32, (EXTRA, dims), 0)
-    for m in range(2):
-        q_own[m, :rows] = queries[m, :rows]
-        line = queries[m, rows:].astype(jnp.float32)[:1]
-        q_own[m, rows:] = jnp.where(extra_row == y, line, 0.0).astype(jnp.bfloat16)
-        q_all[m, nz - 1, y] = q_own[m]
+    for turn in range(1, tp_count):
+        there = lax.rem(mine + turn, tp_count)
+        pl.semaphore_signal(barrier, inc=1, device_id={"tp": there}, device_id_type=MESH)
+
+    for m in range(2):
         got_v[m, 0] = jnp.zeros(got_v.shape[2:], jnp.bfloat16)
         lane = lax.broadcasted_iota(jnp.int32, (8, TILE), 1)
         spot = jnp.where(lane < 4 * blocks, lax.rem(lane, 2 * blocks), lane - 4 * blocks + blocks - 2)
         for h in range(2):
             got_s[m, 0, h] = jnp.where(spot < blocks, HIDDEN, 0.0)
-
-    pl.semaphore_wait(barrier, nz + ny - 2)
+    up = lax.broadcasted_iota(jnp.int32, (TILE, 4 * TILE), 0)
+    right = lax.broadcasted_iota(jnp.int32, (TILE, 4 * TILE), 1)
+    gap = jnp.where(right < 2 * TILE, 2 * up, 2 * up + 2 * TILE + 1)
+    open_up = (gap == right).astype(jnp.float32).astype(jnp.bfloat16)
+
+    for copy in first_loads:
+        copy.wait()
+    place = lax.broadcasted_iota(jnp.int32, (EXTRA, model), 0)
+    low = jnp.broadcast_to(step_token[...].astype(jnp.float32), (EXTRA, model))
+    tokens[rows:] = jnp.where(place == 0, low, 0.0).astype(jnp.bfloat16)
+
+    def norm(i, carry):
+        at = pl.ds(pl.multiple_of(i * EXTRA, EXTRA), EXTRA)
+        floats = tokens[at, :].astype(jnp.float32)
+        inv_rms = lax.rsqrt(jnp.mean(floats * floats, axis=-1, keepdims=True) + EPS)
+        normed[at, :] = (floats * inv_rms * scales[...]).astype(jnp.bfloat16)
+        return carry
+
+    lax.fori_loop(0, tall // EXTRA, norm, 0)
+    for i in range(model // TILE):
+        wider = jnp.dot(normed[:, i * TILE : (i + 1) * TILE], open_up, preferred_element_type=jnp.float32)
+        for m in range(2):
+            part = wider[:, m * 2 * TILE : (m + 1) * 2 * TILE]
+            spaced[m * tall : (m + 1) * tall, i * 2 * TILE : (i + 1) * 2 * TILE] = part.astype(jnp.bfloat16)
+    wq_load.wait()
+    both[...] = jnp.dot(spaced[...], wq[...], preferred_element_type=jnp.float32).astype(jnp.bfloat16)
+    extra_row = lax.broadcasted_iota(jnp.int32, (EXTRA, dims), 0)
+    for m in range(2):
+        q_own[m, :rows] = both[m * tall : m * tall + rows]
+        line = both[m * tall + rows : (m + 1) * tall].astype(jnp.float32)[:1]
+        q_own[m, rows:] = jnp.where(extra_row == y, line, 0.0).astype(jnp.bfloat16)
+        q_all[m, nz - 1, y] = q_own[m]
 
     def to(src, dst, send, recv, device):
         return pltpu.make_async_remote_copy(
@@ -123,9 +176,14 @@
             device_id={"kv": device}, device_id_type=MESH,
         )
 
-    def along_z(m, slot):
-        there = lax.rem(z + (1 + slot if m == 0 else nz - 1 - slot), nz) * ny + y
-        return to(q_own.at[m], q_all.at[m, slot, y], qz_send.at[m, slot], qz_recv.at[m, slot], there)
+    def across(src, dst, send, recv, device):
+        return pltpu.make_async_remote_copy(
+            src_ref=src, dst_ref=dst, send_sem=send, recv_sem=recv,
+            device_id={"tp": device}, device_id_type=MESH,
+        )
+
+    def along_z(m, slot, source):
+        return to(source, q_all.at[m, slot, y], qz_send.at[m, slot], qz_recv.at[m, slot], other_z[m])
 
     def along_y(m, slot, turn, source):
         return to(
@@ -164,42 +222,32 @@
             for i, ref in enumerate((far_v, far_s, far_d))
         )
 
-    for m in range(2):
-        along_z(m, 0).start()
-    for m in range(2):
-        along_z(m, 1).start()
-    for slot in range(2, nz - 1):
+    pl.semaphore_wait(barrier, ny + tp_count)
+    for m in range(2):
+        along_z(m, 0, q_own.at[m]).start()
+
+    def columns_to(turn):
+        there = lax.rem(mine + turn, tp_count)
+        return across(
+            w_out.at[:, pl.ds(pl.multiple_of(there * span, span), span)], cols.at[mine],
+            c_send.at[turn], c_recv.at[turn], there,
+        )
+
+    def pass_on(slot):
         for m in range(2):
-            along_z(m, slot).start()
-    for m in range(2):
-        for turn in range(1, ny):
-            along_y(m, nz - 1, turn, q_own.at[m]).start()
-
-    def fan_out(slot):
-        for m in range(2):
-            along_z(m, slot).wait_recv()
+            along_z(m, slot, q_own.at[m]).wait_recv()
+
+            @pl.when(slot < nz - 2)
+            def _():
+                along_z(m, slot + 1, q_all.at[m, slot, y]).start()
+
             for turn in range(1, ny):
                 along_y(m, slot, turn, q_all.at[m, slot, y]).start()
 
-    fan_out(0)
-
-    key_lane = lax.broadcasted_iota(jnp.int32, (1, cached), 1)
-    bias[...] = jnp.where(me * cached + key_lane < prompt_len[0], 0.0, HIDDEN)
-    values[cached : cached + rows] = new_values[:rows]
-    values[cached + rows :] = jnp.zeros((total_keys - cached - rows, wide), jnp.bfloat16)
-    for m in range(2):
-        fresh = jnp.concatenate(
-            [new_keys[m, :rows].astype(jnp.float32), jnp.zeros((TILE - rows, dims), jnp.float32)], axis=0
-        )
-        kt[m, :, cached:] = jnp.transpose(fresh).astype(jnp.bfloat16)
     up = lax.broadcasted_iota(jnp.int32, (2 * TILE, 2 * TILE), 0)
-    across = lax.broadcasted_iota(jnp.int32, (2 * TILE, 2 * TILE), 1)
-    sort = jnp.where(across < TILE, 2 * across, 2 * across - 2 * TILE + 1) == up
+    right = lax.broadcasted_iota(jnp.int32, (2 * TILE, 2 * TILE), 1)
+    sort = jnp.where(right < TILE, 2 * right, 2 * right - 2 * TILE + 1) == up
     sort = sort.astype(jnp.float32).astype(jnp.bfloat16)
-    up = lax.broadcasted_iota(jnp.int32, (2 * TILE, TILE), 0)
-    across = lax.broadcasted_iota(jnp.int32, (2 * TILE, TILE), 1)
-    halves[...] = (up // 2 == across).astype(jnp.float32).astype(jnp.bfloat16)
-    loads[0].wait()
 
     def split(i, carry):
         block = pairs[pl.ds(pl.multiple_of(i * 2 * TILE, 2 * TILE), 2 * TILE), :]
@@ -211,8 +259,32 @@
         kt[1, :, at] = turned[:, TILE:]
         return carry
 
-    lax.fori_loop(0, cached // TILE, split, 0)
-    for copy in loads[1:]:
+    wk_load.wait()
+    made = jnp.dot(spaced[...], wk[...], preferred_element_type=jnp.float32).astype(jnp.bfloat16)
+    for m in range(2):
+        new_keys[m] = made[m * tall : (m + 1) * tall]
+    pairs_load.wait()
+    lax.fori_loop(0, cached // TILE // 2, split, 0)
+    pass_on(0)
+    wv_load.wait()
+    new_values[...] = jnp.dot(normed[...], wv[...], preferred_element_type=jnp.float32).astype(jnp.bfloat16)
+    lax.fori_loop(cached // TILE // 2, cached // TILE, split, 0)
+    pass_on(1)
+    for turn in range(1, tp_count):
+        columns_to(turn).start()
+    key_lane = lax.broadcasted_iota(jnp.int32, (1, cached), 1)
+    bias[...] = jnp.where(me * cached + key_lane < prompt_len[...], 0.0, HIDDEN)
+    values[cached : cached + rows] = new_values[:rows]
+    values[cached + rows :] = jnp.zeros((total_keys - cached - rows, wide), jnp.bfloat16)
+    for m in range(2):
+        fresh = jnp.concatenate(
+            [new_keys[m, :rows].astype(jnp.float32), jnp.zeros((TILE - rows, dims), jnp.float32)], axis=0
+        )
+        kt[m, :, cached:] = jnp.transpose(fresh).astype(jnp.bfloat16)
+    up = lax.broadcasted_iota(jnp.int32, (2 * TILE, TILE), 0)
+    right = lax.broadcasted_iota(jnp.int32, (2 * TILE, TILE), 1)
+    halves[...] = (up // 2 == right).astype(jnp.float32).astype(jnp.bfloat16)
+    for copy in last_loads:
         copy.wait()
 
     def score(m, h, slot, off):
@@ -311,18 +383,16 @@
     units = [(m, h) for m in range(2) for h in range(2)]
 
     def turn_step(slot, carry):
-        @pl.when(slot < nz - 2)
-        def _():
-            fan_out(slot + 1)
-
-        for m in range(2):
-            for turn in range(1, ny):
-                from_y(m, slot, turn).wait_recv()
+        for turn in range(1, ny):
+            from_y(0, slot, turn).wait_recv()
         homes = [lax.rem(z + nz - 1 - slot, nz), lax.rem(z + 1 + slot, nz)]
         offs = [[(homes[m] * ny + 2 * h - me) * rows for h in range(2)] for m in range(2)]
         tops = [None] * len(units)
         tops[0] = score(0, 0, slot, offs[0][0])
         for u, (m, h) in enumerate(units):
+            if u == 1:
+                for turn in range(1, ny):
+                    from_y(1, slot, turn).wait_recv()
             if u + 1 < len(units):
                 m2, h2 = units[u + 1]
                 tops[u + 1] = score(m2, h2, slot, offs[m2][h2])
@@ -346,6 +416,17 @@
                 for copy in ring(m, slot, h):
                     copy.start()
 
+            if u == 1:
+                @pl.when(slot < nz - 3)
+                def _():
+                    pass_on(slot + 2)
+
+                @pl.when(slot == nz - 3)
+                def _():
+                    for m2 in range(2):
+                        for turn in range(1, ny):
+                            along_y(m2, nz - 1, turn, q_own.at[m2]).start()
+
             @pl.when(slot == nz - 1)
             def _():
                 for there in range(ny):
@@ -386,10 +467,10 @@
                 [spread(s, 4 * blocks + 2, 2, wide) for s in stats],
             )
         )
-    lines = mix_maps(maps_out[0], maps_out[1], ratio[0, 0], gain[...]).astype(jnp.float32)
+    lines = mix_maps(maps_out[0], maps_out[1], ratio[...], gain[...]).astype(jnp.float32)
     place = lax.broadcasted_iota(jnp.int32, lines.shape, 0)
     line = jnp.sum(jnp.where(place == y, lines, 0.0), axis=0, keepdims=True)
-    out[rows:, :] = jnp.where(place == 0, line, 0.0).astype(jnp.bfloat16)
+    heads[mine, rows:] = jnp.where(place == 0, line, 0.0).astype(jnp.bfloat16)
 
     stats = [
         [own_half(sent_s[m, nz - 1, y // 2])] + [own_half(far_s[m, there, y // 2]) for there in peers]
@@ -410,7 +491,21 @@
                     [spread(s, blocks + first, cut // 8, wide) for s in stats[m]],
                 )
             )
-        out[j * cut : (j + 1) * cut, :] = mix_maps(maps_out[0], maps_out[1], ratio[0, 0], gain[...])
+        heads[mine, j * cut : (j + 1) * cut] = mix_maps(maps_out[0], maps_out[1], ratio[...], gain[...])
+
+    def heads_to(turn):
+        there = lax.rem(chip + turn, chips) * 2 + core
+        return across(heads.at[mine], heads.at[mine], h_send.at[turn], h_recv.at[turn], there)
+
+    def heads_over(turn):
+        whose = lax.rem(chip + chips - turn, chips) * 2 + core
+        return across(
+            heads.at[whose], heads.at[whose], d_send.at[turn], d_recv.at[turn], chip * 2 + 1 - core
+        )
+
+    for turn in (2, 1, 3):
+        heads_to(turn).start()
+    heads_over(0).start()
 
     for m in range(2):
         for there in range(ny):
@@ -423,7 +518,7 @@
 
     def drain(slot, carry):
         for m in range(2):
-            along_z(m, slot).wait_send()
+            along_z(m, slot, q_own.at[m]).wait_send()
             for turn in range(1, ny):
                 along_y(m, slot, turn, q_own.at[m]).wait_send()
             for h in range(2):
@@ -432,32 +527,70 @@
         return carry
 
     lax.fori_loop(0, nz - 1, drain, 0)
+    for turn in range(1, tp_count):
+        columns_to(turn).wait()
+
+    def term(whose):
+        return jnp.dot(heads[whose], cols[whose], preferred_element_type=jnp.float32)
+
+    total = term(mine)
+    heads_over(0).wait_recv()
+    total = total + term(chip * 2 + 1 - core)
+    for turn in (1, 3, 2):
+        heads_to(turn).wait_recv()
+        heads_over(turn).start()
+        total = total + term(lax.rem(chip + chips - turn, chips) * 2 + core)
+    for turn in (1, 3, 2):
+        heads_over(turn).wait_recv()
+        total = total + term(lax.rem(chip + chips - turn, chips) * 2 + 1 - core)
+    piece_out[...] = total[:rows].astype(jnp.bfloat16)
+    step_out[...] = total[rows:][:1].astype(jnp.bfloat16)
+    for turn in range(chips):
+        if turn > 0:
+            heads_to(turn).wait_send()
+        heads_over(turn).wait_send()
 
 
 def ring_attend(
-    ratio, prompt_len, step_lens, gain, queries, new_keys, new_values,
-    prompt_keys, prompt_values, cache_keys, cache_values, kv_count, collective,
+    step_lens, ratio, prompt_len, gain, piece, step, scale_in, w_query, w_key, w_value,
+    prompt_keys, prompt_values, cache_keys, cache_values, w_out, kv_count, tp_count, collective,
 ):
-    tall, dims = queries.shape[1:]
-    rows = tall - EXTRA
-    wide = new_values.shape[1]
+    rows, model = piece.shape
+    tall = rows + EXTRA
+    dims = w_query.shape[1]
+    wide = w_value.shape[1]
     cached = prompt_values.shape[0]
     keys = cached + TILE
     ny = SIDE_Y
     nz = kv_count // ny
     deep = ny * rows + EXTRA
+    span = w_out.shape[1] // tp_count
     smem = pl.BlockSpec(memory_space=pltpu.SMEM)
     vmem = pl.BlockSpec(memory_space=pltpu.VMEM)
-    far = pl.BlockSpec(memory_space=pl.ANY)
+    far = pl.BlockSpec(memory_space=pltpu.MemorySpace.HBM)
     dma = pltpu.SemaphoreType.DMA
     half = jnp.bfloat16
     fold = dims ** (-0.5) * math.log2(math.e)
     return pl.pallas_call(
-        functools.partial(ring_kernel, kv_count, fold),
-        out_shape=jax.ShapeDtypeStruct((tall, wide), half),
-        in_specs=[smem] * 3 + [vmem] * 4 + [far] * 4,
-        out_specs=vmem,
+        functools.partial(ring_kernel, kv_count, tp_count, fold),
+        out_shape=[
+            jax.ShapeDtypeStruct((rows, span), half),
+            jax.ShapeDtypeStruct((1, span), half),
+            jax.ShapeDtypeStruct((2, tall, dims), half),
+            jax.ShapeDtypeStruct((tall, wide), half),
+        ],
+        in_specs=[smem] + [vmem] * 3 + [far] * 11,
+        out_specs=[vmem] * 4,
         scratch_shapes=[
+            pltpu.VMEM((tall, model), half),
+            pltpu.VMEM(step.shape, half),
+            pltpu.VMEM(scale_in.shape, jnp.float32),
+            pltpu.VMEM(w_query.shape, half),
+            pltpu.VMEM(w_key.shape, half),
+            pltpu.VMEM(w_value.shape, half),
+            pltpu.VMEM((tall, model), half),
+            pltpu.VMEM((2 * tall, 2 * model), half),
+            pltpu.VMEM((2 * tall, dims), half),
             pltpu.VMEM((2, tall, dims), half),
             pltpu.VMEM((2, nz, ny, tall, dims), half),
             pltpu.VMEM(prompt_keys.shape, half),
@@ -476,96 +609,25 @@
             pltpu.VMEM((2, ny, rows, wide), half),
             pltpu.VMEM((2, ny, 2, 8, TILE), jnp.float32),
             pltpu.VMEM((2, ny, EXTRA, wide), half),
-            dma((4,)),
+            pltpu.VMEM((tp_count, wide, span), half),
+            pltpu.VMEM((tp_count, tall, wide), half),
+            dma((11,)),
             dma((2, nz)), dma((2, nz)),
             dma((2, nz, ny)), dma((2, nz, ny)),
             dma((2, nz, 2, 2)), dma((2, nz, 2, 2)),
             dma((2, ny, 3)), dma((2, ny, 3)),
+            dma((tp_count,)), dma((tp_count,)),
+            dma((tp_count // 2,)), dma((tp_count // 2,)),
+            dma((tp_count // 2,)), dma((tp_count // 2,)),
         ],
         compiler_params=pltpu.CompilerParams(
-            collective_id=collective, has_side_effects=True, vmem_limit_bytes=56 * 1024 * 1024
+            collective_id=collective, has_side_effects=True, vmem_limit_bytes=62 * 1024 * 1024
         ),
         name="ring_attend",
     )(
-        ratio, prompt_len, step_lens, gain, queries, new_keys, new_values,
-        prompt_keys, prompt_values, cache_keys, cache_values,
+        step_lens, ratio, prompt_len, gain, piece, step, scale_in, w_query, w_key, w_value,
+        prompt_keys, prompt_values, cache_keys, cache_values, w_out,
     )
-
-
-def project_out_kernel(axis, count, heads, weight, out, terms, pair, half, far, d_send, d_recv, x_send, x_recv):
-    me = lax.axis_index(axis)
-    chips = count // 2
-    chip, core = me // 2, lax.rem(me, 2)
-    meet(axis, count)
-    wide = out.shape[1]
-    for target in range(count):
-        terms[target] = jnp.dot(
-            heads[...], weight[:, target * wide : target * wide + wide], preferred_element_type=jnp.float32
-        ).astype(jnp.bfloat16)
-    near = []
-    for turn in range(1, chips + 1):
-        there = lax.rem(chip + turn, chips)
-        copy = pltpu.make_async_remote_copy(
-            src_ref=terms.at[there * 2 + 1 - core],
-            dst_ref=pair.at[there],
-            send_sem=d_send.at[turn],
-            recv_sem=d_recv.at[turn],
-            device_id={axis: chip * 2 + 1 - core},
-            device_id_type=MESH,
-        )
-        copy.start()
-        near.append(copy)
-    away = []
-    for turn in range(1, chips + 1):
-        near[turn - 1].wait()
-        there = lax.rem(chip + turn, chips)
-        both = terms[there * 2 + core].astype(jnp.float32) + pair[there].astype(jnp.float32)
-        if turn == chips:
-            total = both
-            for copy in away:
-                copy.wait()
-            for slot in range(1, chips):
-                total = total + far[slot].astype(jnp.float32)
-            out[...] = total.astype(jnp.bfloat16)
-        else:
-            half[turn] = both.astype(jnp.bfloat16)
-            copy = pltpu.make_async_remote_copy(
-                src_ref=half.at[turn],
-                dst_ref=far.at[turn],
-                send_sem=x_send.at[turn],
-                recv_sem=x_recv.at[turn],
-                device_id={axis: there * 2 + core},
-                device_id_type=MESH,
-            )
-            copy.start()
-            away.append(copy)
-
-
-def project_out(heads, weight, axis, count, collective):
-    wide = weight.shape[1] // count
-    rows = heads.shape[0]
-    chips = count // 2
-    vmem = pl.BlockSpec(memory_space=pltpu.VMEM)
-    return pl.pallas_call(
-        functools.partial(project_out_kernel, axis, count),
-        out_shape=jax.ShapeDtypeStruct((rows, wide), jnp.bfloat16),
-        in_specs=[vmem, vmem],
-        out_specs=vmem,
-        scratch_shapes=[
-            pltpu.VMEM((count, rows, wide), jnp.bfloat16),
-            pltpu.VMEM((chips, rows, wide), jnp.bfloat16),
-            pltpu.VMEM((chips, rows, wide), jnp.bfloat16),
-            pltpu.VMEM((chips, rows, wide), jnp.bfloat16),
-            pltpu.SemaphoreType.DMA((chips + 1,)),
-            pltpu.SemaphoreType.DMA((chips + 1,)),
-            pltpu.SemaphoreType.DMA((chips + 1,)),
-            pltpu.SemaphoreType.DMA((chips + 1,)),
-        ],
-        compiler_params=pltpu.CompilerParams(
-            collective_id=collective, has_side_effects=True, vmem_limit_bytes=56 * 1024 * 1024
-        ),
-        name="project_out",
-    )(heads, weight)
 
 
 def on_device(
@@ -591,39 +653,35 @@
     step_dev = step_tokens.shape[0]
     heads, maps, dims = w_query.shape[1:]
     wide = w_value.shape[-1]
-    padded = -(-(piece_dev + step_dev) // EXTRA) * EXTRA
-    spare = jnp.zeros((padded - piece_dev - step_dev, piece_tokens.shape[1]), jnp.bfloat16)
-    all_rows = jnp.concatenate([piece_tokens, step_tokens, spare], axis=0)
-    normed = norm_rows(all_rows, in_gain)
-    queries = project(normed, w_query)
-    key_rows = project(normed, w_key)
-    value_rows = project(normed, w_value)
-    end = piece_dev + step_dev
-
-    def rows_of(flat, start, stop, extra):
-        return jnp.transpose(flat[:, start:stop], (1, 0, 2)).reshape((stop - start,) + extra)
-
-    piece_k = rows_of(key_rows, 0, piece_dev, (heads, maps, dims))
-    step_k = rows_of(key_rows, piece_dev, end, (heads, maps, dims))
-    piece_v = rows_of(value_rows, 0, piece_dev, (heads, wide))
-    step_v = rows_of(value_rows, piece_dev, end, (heads, wide))
-    flat_heads = ring_attend(
+    mixed, line, key_rows, value_rows = ring_attend(
+        step_lens,
         mix_ratio[None, :],
-        prompt_len,
-        step_lens,
+        prompt_len[None, :],
         out_gain[None, :],
-        queries,
-        key_rows,
-        value_rows[0],
+        piece_tokens,
+        step_tokens,
+        in_gain[None, :],
+        w_query.reshape(-1, dims),
+        w_key.reshape(-1, dims),
+        w_value.reshape(-1, wide),
         prompt_keys.reshape(-1, dims),
         prompt_values.reshape(-1, wide),
         step_cache_keys.reshape(-1, dims),
         step_cache_values.reshape(-1, wide),
+        w_out.reshape(-1, w_out.shape[-1]),
         kv_count,
-        1,
+        tp_count,
+        0,
     )
-    mixed = project_out(flat_heads, w_out.reshape(-1, w_out.shape[-1]), "tp", tp_count, 2)
-    return (mixed[:piece_dev], mixed[piece_dev:end], piece_k, piece_v, step_k, step_v)
+    piece_out, step_out, piece_k, piece_v, step_k, step_v = finish(mixed, line, key_rows, value_rows)
+    return (
+        piece_out,
+        step_out,
+        piece_k.reshape(piece_dev, heads, maps, dims),
+        piece_v.reshape(piece_dev, heads, wide),
+        step_k.reshape(step_dev, heads, maps, dims),
+        step_v.reshape(step_dev, heads, wide),
+    )
 
 
 def solution(mesh):

time: 102 us -> 81.7 us (0.80)
  Pallas kernels: 87.5 us -> 79.6 us
  local copies, waits for them, and re-layouts: 5.8 us -> 0 us
  matrix products: 4.98 us -> 0 us
  other arithmetic: 1.68 us -> 0 us
    pallas_call x2, Pallas kernels: 87.5 us -> 79.6 us  [the longest x1 77.9 us: ring_attend(): pl.pallas_call(functools.partial(ring_kernel, kv_count, tp_count, fold),...]
    dot_general x3 -> x0, matrix products: 4.98 us -> none  [project(): jnp.einsum('nd,gdk->gnk', normed, parts, preferred_element_type=jnp.float32)]
    slice x4 -> x0, local copies, waits for them, and re-layouts: 3.39 us -> none  [the longest x1 1.54 us: on_device(): mixed[:piece_dev]]
    unnamed x18 -> x0, local copies, waits for them, and re-layouts: 1.71 us -> none
    reduce_sum x1 -> x0, other arithmetic: 1.67 us -> none  [norm_rows(): inv_rms = lax.rsqrt(jnp.mean(floats * floats, axis=-1, keepdims=True) + EPS)]
where the time goes in v3:
time: 81.7 us; the launch traced here: 81.5 us
  Pallas kernels  79.6 us (97%)
  between operations  1.94 us (2%)
    pallas_call x1, Pallas kernels, ring_attend(): pl.pallas_call(functools.partial(ring_kernel, kv_count, tp_count, fold),...  77.9 us
    pallas_call x1, Pallas kernels, finish(): pl.pallas_call(finish_kernel, out_shape=[jax.ShapeDtypeStruct(shape, jnp....  1.69 us

profile of v3, /device:TPU:1, one launch (start us, length us, event | category | flops | bytes accessed | tf_op | source)
XLA Modules:
  0.0 81.5 jit_solution(6483848745710039773)
XLA Ops:
  1.9 77.9 %ring_attend.1 = (bf16[96,512]{1,0:T(8,128)(2,1)}, bf16[1,512]{1,0:T(2,128)(2,1)}, bf16[2,112,128]{2,1,0:T(8,128)(2,1)}, bf16[112,256]{1,0:T(8,128)(2,1)}) custom-call(s32[32]{0:T(128)} %step_lens.1, f32[1,1]{1,0:T(1,128)} %bitcast.18.ratio, s32[1,1]{1,0:T(1,128)} %bitcast.19.prompt_len, f32[1,256]{1,0:T(1,128)} %bitcast.29, bf16[96,4096]{1,0:T(8,128)(2,1)} %piece.1, ...), custom_call_target="tpu_custom_call" | custom-call | tf_op jit(solution)/shard_map/ring_attend/pallas_call | solution.py:574
  79.8 1.7 %finish.1 = (bf16[96,512]{1,0:T(8,128)(2,1)}, bf16[1,512]{1,0:T(2,128)(2,1)}, bf16[192,128]{1,0:T(8,128)(2,1)}, bf16[96,256]{1,0:T(8,128)(2,1)}, bf16[2,128]{1,0:T(2,128)(2,1)}, /*index=5*/bf16[1,256]{1,0:T(2,128)(2,1)}) custom-call(bf16[96,512]{1,0:T(8,128)(2,1)} %get-tuple-element.16.mixed, bf16[1,512]{1,0:T(2,128)(2,1)} %get-tuple-element.17.line, ...), custom_call_target="tpu_custom_call" | custom-call | tf_op jit(solution)/shard_map/finish/pallas_call | solution.py:41

commit v4 on v3

--- a/solution.py
+++ b/solution.py
@@ -125,8 +125,11 @@
     ]
 
     barrier = pltpu.get_barrier_semaphore()
-    for there in other_z + [z * ny + lax.rem(y + turn, ny) for turn in range(1, ny)]:
-        pl.semaphore_signal(barrier, inc=1, device_id={"kv": there}, device_id_type=MESH)
+    sides = [lax.rem(z + 1, nz) * ny, lax.rem(z + nz - 1, nz) * ny]
+    for side in sides + [z * ny]:
+        for turn in range(side is not sides[0] and side is not sides[1], ny):
+            there = side + lax.rem(y + turn, ny)
+            pl.semaphore_signal(barrier, inc=1, device_id={"kv": there}, device_id_type=MESH)
     for turn in range(1, tp_count):
         there = lax.rem(mine + turn, tp_count)
         pl.semaphore_signal(barrier, inc=1, device_id={"tp": there}, device_id_type=MESH)
@@ -159,8 +162,8 @@
     for i in range(model // TILE):
         wider = jnp.dot(normed[:, i * TILE : (i + 1) * TILE], open_up, preferred_element_type=jnp.float32)
         for m in range(2):
-            part = wider[:, m * 2 * TILE : (m + 1) * 2 * TILE]
-            spaced[m * tall : (m + 1) * tall, i * 2 * TILE : (i + 1) * 2 * TILE] = part.astype(jnp.bfloat16)
+            slab = wider[:, m * 2 * TILE : (m + 1) * 2 * TILE]
+            spaced[m * tall : (m + 1) * tall, i * 2 * TILE : (i + 1) * 2 * TILE] = slab.astype(jnp.bfloat16)
     wq_load.wait()
     both[...] = jnp.dot(spaced[...], wq[...], preferred_element_type=jnp.float32).astype(jnp.bfloat16)
     extra_row = lax.broadcasted_iota(jnp.int32, (EXTRA, dims), 0)
@@ -191,6 +194,12 @@
             z * ny + lax.rem(y + turn, ny),
         )
 
+    def across_both(m, turn):
+        return to(
+            q_own.at[m], q_all.at[m, 0, y], qy_send.at[m, 0, turn], qy_recv.at[m, 0, y],
+            sides[m] + lax.rem(y + turn, ny),
+        )
+
     def from_y(m, slot, turn):
         there = lax.rem(y + turn, ny)
         return to(
@@ -222,9 +231,12 @@
             for i, ref in enumerate((far_v, far_s, far_d))
         )
 
-    pl.semaphore_wait(barrier, ny + tp_count)
+    pl.semaphore_wait(barrier, 3 * ny - 1 + tp_count - 1)
     for m in range(2):
         along_z(m, 0, q_own.at[m]).start()
+    for turn in (1, 3, 2):
+        for m in range(2):
+            across_both(m, turn).start()
 
     def columns_to(turn):
         there = lax.rem(mine + turn, tp_count)
@@ -241,8 +253,10 @@
             def _():
                 along_z(m, slot + 1, q_all.at[m, slot, y]).start()
 
-            for turn in range(1, ny):
-                along_y(m, slot, turn, q_all.at[m, slot, y]).start()
+            @pl.when(slot > 0)
+            def _():
+                for turn in range(1, ny):
+                    along_y(m, slot, turn, q_all.at[m, slot, y]).start()
 
     up = lax.broadcasted_iota(jnp.int32, (2 * TILE, 2 * TILE), 0)
     right = lax.broadcasted_iota(jnp.int32, (2 * TILE, 2 * TILE), 1)
@@ -289,7 +303,7 @@
 
     def score(m, h, slot, off):
         q = q_all[m, slot, 2 * h : 2 * h + 2, :rows].reshape(half, dims)
-        buf = (2 * m + h) % 2
+        buf = m
         best = None
         for c in range(0, cached, 256):
             s = jnp.dot(q, kt[m, :, c : c + 256], preferred_element_type=jnp.float32)
@@ -308,7 +322,7 @@
         return jnp.max(best, axis=1, keepdims=True)
 
     def weigh(m, h, top):
-        buf = (2 * m + h) % 2
+        buf = m
         part = None
         for c in range(0, total_keys, TILE):
             w = jnp.exp2((scores[buf, :, c : c + TILE] - top) * fold)
@@ -380,19 +394,17 @@
                 line += 8
         sent_s[m, slot, h] = pack_columns(columns)
 
-    units = [(m, h) for m in range(2) for h in range(2)]
+    units = [(m, h) for h in range(2) for m in range(2)]
 
     def turn_step(slot, carry):
-        for turn in range(1, ny):
-            from_y(0, slot, turn).wait_recv()
+        for m in range(2):
+            for turn in range(1, ny):
+                from_y(m, slot, turn).wait_recv()
         homes = [lax.rem(z + nz - 1 - slot, nz), lax.rem(z + 1 + slot, nz)]
         offs = [[(homes[m] * ny + 2 * h - me) * rows for h in range(2)] for m in range(2)]
         tops = [None] * len(units)
         tops[0] = score(0, 0, slot, offs[0][0])
         for u, (m, h) in enumerate(units):
-            if u == 1:
-                for turn in range(1, ny):
-                    from_y(1, slot, turn).wait_recv()
             if u + 1 < len(units):
                 m2, h2 = units[u + 1]
                 tops[u + 1] = score(m2, h2, slot, offs[m2][h2])
@@ -439,10 +451,6 @@
 
     lax.fori_loop(0, nz, turn_step, 0)
 
-    for m in range(2):
-        for turn in range(1, ny):
-            for copy in final_from(m, lax.rem(y + turn, ny)):
-                copy.wait_recv()
     odd = lax.rem(y, 2) == 1
 
     def own_half(stats):
@@ -456,42 +464,42 @@
         return total / norm
 
     peers = [lax.rem(y + turn, ny) for turn in range(1, ny)]
-    maps_out = []
+    cut = 32
+    gathered = []
     for m in range(2):
-        vals = [sent_v[m, nz - 1, deep:]] + [far_d[m, there] for there in peers]
-        stats = [sent_s[m, nz - 1, 1]] + [far_s[m, there, 1] for there in peers]
-        maps_out.append(
-            merge(
-                vals,
-                [spread(s, 4 * blocks, 2, wide) for s in stats],
-                [spread(s, 4 * blocks + 2, 2, wide) for s in stats],
-            )
-        )
-    lines = mix_maps(maps_out[0], maps_out[1], ratio[...], gain[...]).astype(jnp.float32)
-    place = lax.broadcasted_iota(jnp.int32, lines.shape, 0)
-    line = jnp.sum(jnp.where(place == y, lines, 0.0), axis=0, keepdims=True)
-    heads[mine, rows:] = jnp.where(place == 0, line, 0.0).astype(jnp.bfloat16)
-
-    stats = [
-        [own_half(sent_s[m, nz - 1, y // 2])] + [own_half(far_s[m, there, y // 2]) for there in peers]
-        for m in range(2)
-    ]
-    cut = 32
-    for j in range(rows // cut):
-        maps_out = []
-        for m in range(2):
+        for there in peers:
+            for copy in final_from(m, there):
+                copy.wait_recv()
+        stats = [own_half(sent_s[m, nz - 1, y // 2])] + [own_half(far_s[m, there, y // 2]) for there in peers]
+        parts = []
+        for j in range(rows // cut):
             at = pl.ds(pl.multiple_of(y * rows + j * cut, cut), cut)
             vals = [sent_v[m, nz - 1, at, :]]
             vals += [far_v[m, there, j * cut : (j + 1) * cut, :] for there in peers]
             first = j * cut // 8
-            maps_out.append(
+            parts.append(
                 merge(
                     vals,
-                    [spread(s, first, cut // 8, wide) for s in stats[m]],
-                    [spread(s, blocks + first, cut // 8, wide) for s in stats[m]],
+                    [spread(s, first, cut // 8, wide) for s in stats],
+                    [spread(s, blocks + first, cut // 8, wide) for s in stats],
                 )
             )
-        heads[mine, j * cut : (j + 1) * cut] = mix_maps(maps_out[0], maps_out[1], ratio[...], gain[...])
+        stats = [sent_s[m, nz - 1, 1]] + [far_s[m, there, 1] for there in peers]
+        parts.append(
+            merge(
+                [sent_v[m, nz - 1, deep:]] + [far_d[m, there] for there in peers],
+                [spread(s, 4 * blocks, 2, wide) for s in stats],
+                [spread(s, 4 * blocks + 2, 2, wide) for s in stats],
+            )
+        )
+        gathered.append(parts)
+    mixed = [mix_maps(one, two, ratio[...], gain[...]) for one, two in zip(*gathered)]
+    for j in range(rows // cut):
+        heads[mine, j * cut : (j + 1) * cut] = mixed[j]
+    lines = mixed[-1].astype(jnp.float32)
+    place = lax.broadcasted_iota(jnp.int32, lines.shape, 0)
+    line = jnp.sum(jnp.where(place == y, lines, 0.0), axis=0, keepdims=True)
+    heads[mine, rows:] = jnp.where(place == 0, line, 0.0).astype(jnp.bfloat16)
 
     def heads_to(turn):
         there = lax.rem(chip + turn, chips) * 2 + core

time: 81.7 us -> 80.7 us (0.988)
  Pallas kernels: 79.6 us -> 78.6 us
    pallas_call x1, Pallas kernels: 77.9 us -> 76.9 us  [ring_attend(): pl.pallas_call(functools.partial(ring_kernel, kv_count, tp_count, fold),...]
where the time goes in v4:
time: 80.7 us; the launch traced here: 80.5 us
  Pallas kernels  78.6 us (97%)
  between operations  1.94 us (2%)
    pallas_call x1, Pallas kernels, ring_attend(): pl.pallas_call(functools.partial(ring_kernel, kv_count, tp_count, fold),...  76.9 us
    pallas_call x1, Pallas kernels, finish(): pl.pallas_call(finish_kernel, out_shape=[jax.ShapeDtypeStruct(shape, jnp....  1.69 us

profile of v4, /device:TPU:1, one launch (start us, length us, event | category | flops | bytes accessed | tf_op | source)
XLA Modules:
  0.0 80.5 jit_solution(3580753175432721534)
XLA Ops:
  1.9 76.9 %ring_attend.1 = (bf16[96,512]{1,0:T(8,128)(2,1)}, bf16[1,512]{1,0:T(2,128)(2,1)}, bf16[2,112,128]{2,1,0:T(8,128)(2,1)}, bf16[112,256]{1,0:T(8,128)(2,1)}) custom-call(s32[32]{0:T(128)} %step_lens.1, f32[1,1]{1,0:T(1,128)} %bitcast.18.ratio, s32[1,1]{1,0:T(1,128)} %bitcast.19.prompt_len, f32[1,256]{1,0:T(1,128)} %bitcast.29, bf16[96,4096]{1,0:T(8,128)(2,1)} %piece.1, ...), custom_call_target="tpu_custom_call" | custom-call | tf_op jit(solution)/shard_map/ring_attend/pallas_call | solution.py:582
  78.8 1.7 %finish.1 = (bf16[96,512]{1,0:T(8,128)(2,1)}, bf16[1,512]{1,0:T(2,128)(2,1)}, bf16[192,128]{1,0:T(8,128)(2,1)}, bf16[96,256]{1,0:T(8,128)(2,1)}, bf16[2,128]{1,0:T(2,128)(2,1)}, /*index=5*/bf16[1,256]{1,0:T(2,128)(2,1)}) custom-call(bf16[96,512]{1,0:T(8,128)(2,1)} %get-tuple-element.16.mixed, bf16[1,512]{1,0:T(2,128)(2,1)} %get-tuple-element.17.line, ...), custom_call_target="tpu_custom_call" | custom-call | tf_op jit(solution)/shard_map/finish/pallas_call | solution.py:41

commit v5 on v4

--- a/solution.py
+++ b/solution.py
@@ -56,7 +56,7 @@
 
 SIDE_Y = 4
 TILE = 128
-EXTRA = 16
+EXTRA = 8
 
 
 def spread(stats, first, groups, width):
@@ -137,7 +137,7 @@
     for m in range(2):
         got_v[m, 0] = jnp.zeros(got_v.shape[2:], jnp.bfloat16)
         lane = lax.broadcasted_iota(jnp.int32, (8, TILE), 1)
-        spot = jnp.where(lane < 4 * blocks, lax.rem(lane, 2 * blocks), lane - 4 * blocks + blocks - 2)
+        spot = jnp.where(lane < 4 * blocks, lax.rem(lane, 2 * blocks), lane - 4 * blocks + blocks - EXTRA // 8)
         for h in range(2):
             got_s[m, 0, h] = jnp.where(spot < blocks, HIDDEN, 0.0)
     up = lax.broadcasted_iota(jnp.int32, (TILE, 4 * TILE), 0)
@@ -374,7 +374,7 @@
     def join(m, h, slot, top, total, summed):
         at = pl.ds(h * half, half + h * EXTRA)
         old = got_s[m, slot, h]
-        places = [(2 * blocks * j, blocks) for j in range(2)] + [(4 * blocks, 2)] * h
+        places = [(2 * blocks * j, blocks) for j in range(2)] + [(4 * blocks, EXTRA // 8)] * h
         old_top = jnp.concatenate([spread(old, first, n, TILE) for first, n in places], axis=0)
         old_total = jnp.concatenate([spread(old, first + n, n, TILE) for first, n in places], axis=0)
         best = jnp.maximum(old_top, top)
@@ -488,8 +488,8 @@
         parts.append(
             merge(
                 [sent_v[m, nz - 1, deep:]] + [far_d[m, there] for there in peers],
-                [spread(s, 4 * blocks, 2, wide) for s in stats],
-                [spread(s, 4 * blocks + 2, 2, wide) for s in stats],
+                [spread(s, 4 * blocks, EXTRA // 8, wide) for s in stats],
+                [spread(s, 4 * blocks + EXTRA // 8, EXTRA // 8, wide) for s in stats],
             )
         )
         gathered.append(parts)

time: 80.7 us -> 80.7 us (level)
  no operation moved by 1% of the time
where the time goes in v5:
time: 80.7 us; the launch traced here: 80.5 us
  Pallas kernels  78.6 us (97%)
  between operations  1.94 us (2%)
    pallas_call x1, Pallas kernels, ring_attend(): pl.pallas_call(functools.partial(ring_kernel, kv_count, tp_count, fold),...  76.9 us
    pallas_call x1, Pallas kernels, finish(): pl.pallas_call(finish_kernel, out_shape=[jax.ShapeDtypeStruct(shape, jnp....  1.69 us

profile of v5, /device:TPU:1, one launch (start us, length us, event | category | flops | bytes accessed | tf_op | source)
XLA Modules:
  0.0 80.5 jit_solution(7251471619057976475)
XLA Ops:
  1.9 76.9 %ring_attend.1 = (bf16[96,512]{1,0:T(8,128)(2,1)}, bf16[1,512]{1,0:T(2,128)(2,1)}, bf16[2,104,128]{2,1,0:T(8,128)(2,1)}, bf16[104,256]{1,0:T(8,128)(2,1)}) custom-call(s32[32]{0:T(128)} %step_lens.1, f32[1,1]{1,0:T(1,128)} %bitcast.18.ratio, s32[1,1]{1,0:T(1,128)} %bitcast.19.prompt_len, f32[1,256]{1,0:T(1,128)} %bitcast.29, bf16[96,4096]{1,0:T(8,128)(2,1)} %piece.1, ...), custom_call_target="tpu_custom_call" | custom-call | tf_op jit(solution)/shard_map/ring_attend/pallas_call | solution.py:582
  78.8 1.7 %finish.1 = (bf16[96,512]{1,0:T(8,128)(2,1)}, bf16[1,512]{1,0:T(2,128)(2,1)}, bf16[192,128]{1,0:T(8,128)(2,1)}, bf16[96,256]{1,0:T(8,128)(2,1)}, bf16[2,128]{1,0:T(2,128)(2,1)}, /*index=5*/bf16[1,256]{1,0:T(2,128)(2,1)}) custom-call(bf16[96,512]{1,0:T(8,128)(2,1)} %get-tuple-element.16.mixed, bf16[1,512]{1,0:T(2,128)(2,1)} %get-tuple-element.17.line, ...), custom_call_target="tpu_custom_call" | custom-call | tf_op jit(solution)/shard_map/finish/pallas_call | solution.py:41
